TPU v7x, 256 devices: a 8x8x2 block of a 8x8x16 slice. The times are simulated.
256 devices in a mesh: grp: 2 (over z), st: 16 (over y, core), tp: 8 (over x).
Axes of the slice: x: 8, y: 8, z: 2, core: 2. Of those that a mesh axis runs over, the one named last changes fastest.
The devices are a block of a 8x8x16 slice.
Arguments:
- tokens: bfloat16 [16384, 2048], P(('grp', 'st')), parts along dimension 0, may hold values from -6 to 6, as said below
- store: bfloat16 [256, 128, 2048], P(('grp', 'st')), parts along dimension 0, may hold values from -6 to 6, as said below
- passage_ids: int32 [256, 4], P(('grp', 'st')), parts along dimension 0, may hold values from 0 to 127, as said below
- mix_gain: float32 [2048], replicated, may hold values from 0.1 to 1.9
- glu_value: bfloat16 [2048, 1024], P(None, 'tp'), may hold values from -0.125 to 0.125
- glu_gate: bfloat16 [2048, 1024], P(None, 'tp'), may hold values from -0.125 to 0.125
- conv_taps: bfloat16 [31, 1024], P(None, 'tp'), may hold values from -5 to 5
- channel_gain: float32 [1024], P('tp'), may hold values from 0.1 to 1.9
- mix_out: bfloat16 [1024, 2048], P('tp'), may hold values from -0.1875 to 0.1875
- query_gain: float32 [2048], replicated, may hold values from 0.1 to 1.9
- passage_gain: float32 [2048], replicated, may hold values from 0.1 to 1.9
- query_proj: bfloat16 [2048, 2048], P(None, 'tp'), may hold values from -1 to 1
- key_proj: bfloat16 [2048, 2048], P(None, 'tp'), may hold values from -1 to 1
- value_proj: bfloat16 [2048, 2048], P(None, 'tp'), may hold values from -0.125 to 0.125
- attn_out: bfloat16 [2048, 2048], P('tp'), may hold values from -0.125 to 0.125
- blend_gain: float32 [2048], replicated, may hold values from 0.5 to 3
Outputs:
- blended: bfloat16 [16384, 2048], P(('grp', 'st', 'tp')), parts along dimension 0
There are 2 independent parts, one for each index of `grp`. A program takes and returns all parts, laid end to end along the dimension named above; an argument that names none is the same for every part. Nothing has to cross between parts.
Inputs may be any that keep to these rules, and one draw needn't show every extreme that they name: `tokens`: standard normal entries clipped to the range. `store`: standard normal entries clipped to the range. `passage_ids`: passage p is held by index p // 8 of st. The 32 requests of the 8 blocks of one index of st (repeats counted) name at most 4 passages held by any one index of st, and in every draw one index of st receives exactly 4 requests from every index of st.
All inputs are finite; a program needn't handle non-finite values.
Results may differ from a plain program's by a relative error of at most 0.01575.
The roundings to bfloat16 on the way count: a program that leaves them out, or rounds other values in their place, can miss the bound.
Values may be sent and summed in bfloat16 or wider, within the bound.
A program may use at most 128 MiB of HBM per device.

v0:
```python
import jax
import jax.numpy as jnp
from jax import lax
from jax.sharding import PartitionSpec as P

CA = 1024
HD = 256
SEQ_LEN = 128


EPS = 1e-06


def side_by_side(arrays, axis, split_dim, concat_dim, along):
    widths = [a.shape[along] for a in arrays]
    both = jnp.concatenate(arrays, axis=along)
    out = lax.all_to_all(both, axis, split_axis=split_dim, concat_axis=concat_dim, tiled=True)
    return tuple(jnp.split(out, [sum(widths[:k]) for k in range(1, len(widths))], axis=along))


def cut_along(x, dim, size):
    dims = x.shape
    pieces = x.reshape(*dims[:dim], size, dims[dim] // size, *dims[dim + 1 :])
    return jnp.moveaxis(pieces, dim, 0)


def sent_and_summed(x, axis, dim):
    size = lax.axis_size(axis)
    pieces = lax.all_to_all(cut_along(x, dim, size), axis, 0, 0, tiled=True)
    return jnp.sum(pieces.astype(jnp.float32), axis=0)


def rms_rows(row_data, gain_vec):
    floats = row_data.astype(jnp.float32)
    inv_scale = lax.rsqrt(jnp.mean(floats * floats, axis=-1, keepdims=True) + EPS)
    return (floats * inv_scale * gain_vec).astype(jnp.bfloat16)


def depthwise(gated_rows, conv_taps):
    span_width = conv_taps.shape[0]
    half_span = (span_width - 1) // 2
    seq_length = gated_rows.shape[1]
    padded = jnp.pad(
        gated_rows.astype(jnp.float32), ((0, 0), (half_span, span_width - 1 - half_span), (0, 0))
    )
    running = jnp.zeros(gated_rows.shape, jnp.float32)
    for tap_index in range(span_width):
        running = running + padded[:, tap_index : tap_index + seq_length] * conv_taps[
            tap_index
        ].astype(jnp.float32)
    return running


def passage_attention(queries, keys_values, head_count):
    groups, block_len, span_width = queries.shape
    head_dim = span_width // head_count
    row_count = keys_values.shape[1]
    query_heads = queries.reshape(groups, block_len, head_count, head_dim)
    key_heads = keys_values[:, :, :span_width].reshape(groups, row_count, head_count, head_dim)
    value_heads = keys_values[:, :, span_width:].reshape(groups, row_count, head_count, head_dim)
    scores = jnp.einsum(
        "gqhd,grhd->ghqr", query_heads, key_heads, preferred_element_type=jnp.float32
    ) * head_dim ** (-0.5)
    row_top = jnp.max(scores, axis=-1)
    exponent = jnp.exp(scores - row_top[..., None])
    row_sum = jnp.sum(exponent, axis=-1)
    weights = exponent.astype(jnp.bfloat16)
    outputs = jnp.einsum(
        "ghqr,grhd->gqhd", weights, value_heads, preferred_element_type=jnp.float32
    ).astype(jnp.bfloat16)
    return (outputs.reshape(groups, block_len, span_width), row_top, row_sum)


def combine(outs, tops, sums, head_count):
    batch_count, passage_count, block_len, span_width = outs.shape
    head_dim = span_width // head_count
    best_top = jnp.max(tops, axis=1, keepdims=True)
    weight = jnp.exp(tops - best_top)
    numerator = jnp.einsum(
        "bphq,bpqhd->bqhd",
        weight,
        outs.astype(jnp.float32).reshape(
            batch_count, passage_count, block_len, head_count, head_dim
        ),
    )
    denominator = jnp.sum(weight * sums, axis=1)
    result = numerator / jnp.transpose(denominator, (0, 2, 1))[..., None]
    return result.reshape(batch_count, block_len, span_width).astype(jnp.bfloat16)


def local(
    tokens,
    store,
    passage_ids,
    mix_gain,
    glu_value,
    glu_gate,
    conv_taps,
    channel_gain,
    mix_out,
    query_gain,
    passage_gain,
    query_proj,
    key_proj,
    value_proj,
    attn_out,
    blend_gain,
):
    owners = lax.axis_size("st")
    tok_rows = tokens.shape[0]
    model_width = tokens.shape[1]
    local_channels = glu_value.shape[1]
    head_width = query_proj.shape[1]
    local_heads = head_width // HD
    block_count = passage_ids.shape[0]
    per_block = passage_ids.shape[1]
    block_len = tok_rows // block_count
    requests = block_count * per_block
    capacity = 2 * requests // owners
    pass_local = store.shape[0]
    pass_rows = store.shape[1]
    flat_ids = passage_ids.reshape(requests)
    owner_of = flat_ids // pass_local
    local_of = flat_ids - owner_of * pass_local
    request_index = jnp.arange(requests)
    earlier = (owner_of[:, None] == owner_of[None, :]) & (
        request_index[None, :] < request_index[:, None]
    )
    ranking = jnp.sum(earlier.astype(jnp.int32), axis=1)
    slot_of = owner_of * capacity + ranking
    slot_ids = (
        jnp.zeros((owners * capacity,), jnp.int32)
        .at[slot_of]
        .set(local_of)
        .reshape(owners, capacity)
    )
    asked = lax.all_to_all(slot_ids, "st", split_axis=0, concat_axis=0, tiled=True)
    normed_store = rms_rows(store.reshape(pass_local * pass_rows, model_width), passage_gain)
    key_rows = jnp.dot(normed_store, key_proj, preferred_element_type=jnp.float32).astype(
        jnp.bfloat16
    )
    value_rows = jnp.dot(normed_store, value_proj, preferred_element_type=jnp.float32).astype(
        jnp.bfloat16
    )
    memory = jnp.concatenate([key_rows, value_rows], axis=1).reshape(
        pass_local, pass_rows, 2 * head_width
    )
    queries = jnp.dot(
        rms_rows(tokens, query_gain), query_proj, preferred_element_type=jnp.float32
    ).astype(jnp.bfloat16)
    query_blocks = queries.reshape(block_count, block_len, head_width)
    repeated = jnp.repeat(query_blocks, per_block, axis=0)
    served = memory[asked.reshape(owners * capacity)]
    slot_queries = (
        jnp.zeros((owners * capacity, block_len, head_width), jnp.bfloat16)
        .at[slot_of]
        .set(repeated)
    )
    visiting = lax.all_to_all(
        slot_queries.reshape(owners, capacity, block_len, head_width),
        "st",
        split_axis=0,
        concat_axis=0,
        tiled=True,
    )
    answer_out, answer_top, answer_sum = passage_attention(
        visiting.reshape(owners * capacity, block_len, head_width), served, local_heads
    )
    back_out = lax.all_to_all(
        answer_out.reshape(owners, capacity, block_len, head_width),
        "st",
        split_axis=0,
        concat_axis=0,
        tiled=True,
    )
    back_top, back_sum = side_by_side(
        (
            answer_top.reshape(owners, capacity, local_heads, block_len),
            answer_sum.reshape(owners, capacity, local_heads, block_len),
        ),
        "st",
        0,
        0,
        1,
    )
    partial_out = back_out.reshape(owners * capacity, block_len, head_width)[slot_of]
    partial_top = back_top.reshape(owners * capacity, local_heads, block_len)[slot_of]
    partial_sum = back_sum.reshape(owners * capacity, local_heads, block_len)[slot_of]
    attended = combine(
        partial_out.reshape(block_count, per_block, block_len, head_width),
        partial_top.reshape(block_count, per_block, local_heads, block_len),
        partial_sum.reshape(block_count, per_block, local_heads, block_len),
        local_heads,
    ).reshape(tok_rows, head_width)
    mix_input = rms_rows(tokens, mix_gain)
    value_part = jnp.dot(mix_input, glu_value, preferred_element_type=jnp.float32)
    gate_part = jnp.dot(mix_input, glu_gate, preferred_element_type=jnp.float32)
    gated_rows = (value_part * jax.nn.sigmoid(gate_part)).astype(jnp.bfloat16)
    conv_rows = depthwise(gated_rows.reshape(-1, SEQ_LEN, local_channels), conv_taps).reshape(
        tok_rows, local_channels
    )
    channel_sum, channel_square = lax.psum(
        (jnp.sum(conv_rows, axis=1), jnp.sum(conv_rows * conv_rows, axis=1)), "tp"
    )
    row_mean = channel_sum / CA
    row_var = channel_square / CA - row_mean * row_mean
    activation = jax.nn.silu(
        (conv_rows - row_mean[:, None]) * lax.rsqrt(row_var + EPS)[:, None] * channel_gain
    ).astype(jnp.bfloat16)
    conv_term = jnp.dot(activation, mix_out, preferred_element_type=jnp.float32)
    attn_term = jnp.dot(attended, attn_out, preferred_element_type=jnp.float32)
    summed = sent_and_summed((conv_term + blend_gain * attn_term).astype(jnp.bfloat16), "tp", 0)
    return summed.astype(jnp.bfloat16)


def solution(mesh):
    in_specs = (
        P(("grp", "st"), None),
        P(("grp", "st"), None, None),
        P(("grp", "st"), None),
        P(),
        P(None, "tp"),
        P(None, "tp"),
        P(None, "tp"),
        P("tp"),
        P("tp", None),
        P(),
        P(),
        P(None, "tp"),
        P(None, "tp"),
        P(None, "tp"),
        P("tp", None),
        P(),
    )
    out_specs = P(("grp", "st", "tp"), None)
    return jax.shard_map(local, mesh=mesh, in_specs=in_specs, out_specs=out_specs, check_vma=False)
```

profile of v0, /device:TPU:528, one launch (start us, length us, event | category | flops | bytes accessed | tf_op | source)
XLA Modules:
  0.0 223.9 jit_solution(15282987178390974926)
XLA Ops:
  0.0 0.8 copy.26
  1.0 0.2 convert_reduce_fusion
  1.2 0.7 scatter_custom_fusion.1
  1.9 0.7 all_to_all.19
  2.6 21.5 %all-to-all-start.1 = ((s32[16,1,4]{2,1,0:T(1,128)}), s32[16,1,4]{2,1,0:T(1,128)S(1)}, u32[]{:S(2)}, u32[]{:S(2)}) async-start(s32[16,1,4]{2,1,0:T(1,128)} %bitcast.45), calls=%async_computation.1 | async-start | bytes 16384 | tf_op jit(solution)/shard_map/all_to_all | solution.py:137
  24.1 2.1 fusion.6
  26.2 2.6 %fusion.20 = bf16[512,256]{1,0:T(8,128)(2,1)S(1)} fusion(bf16[2048,256]{1,0:T(8,128)(2,1)} %param.27, bf16[512,2048]{1,0:T(8,128)(2,1)} %param.16, f32[2048]{0:T(1024)} %param.25, f32[512]{0:T(512)S(1)} %add_rsqrt_fusion.1), kind=kOutput, calls=%fused_computation.32 | convolution fusion | flops 541196288 | bytes 3418112 | tf_op jit(solution)/shard_map/dot_general | solution.py:148
  28.9 0.1 broadcast_in_dim.5
  29.0 1.6 broadcast_in_dim.4
  30.5 4.6 %scatter_fusion = bf16[64,64,256]{2,1,0:T(8,128)(2,1)} fusion(bf16[64,64,256]{2,1,0:T(8,128)(2,1)} %broadcast_in_dim.4, s32[32]{0:T(128)S(1)} %fusion.100, bf16[32,64,256]{2,1,0:T(8,128)(2,1)S(1)} %bitcast.174), kind=kCustom, calls=%fused_computation.4 | custom fusion | bytes 3145856 | tf_op jit(solution)/shard_map/scatter | solution.py:157
  35.1 7.5 %all-to-all-start = ((bf16[16,4,64,256]{3,2,1,0:T(8,128)(2,1)}), bf16[16,4,64,256]{3,2,1,0:T(8,128)(2,1)}, u32[]{:S(2)}, u32[]{:S(2)}) async-start(bf16[16,4,64,256]{3,2,1,0:T(8,128)(2,1)} %bitcast.40), calls=%async_computation | async-start | bytes 4194304 | tf_op jit(solution)/shard_map/all_to_all | solution.py:159
  42.6 3.2 %multiply_reduce_fusion = f32[8,128]{1,0:T(8,128)S(1)} fusion(bf16[8,128,2048]{2,1,0:T(8,128)(2,1)} %param.17), kind=kLoop, calls=%fused_computation.9 | loop fusion | flops 6290432 | bytes 4198400 | tf_op jit(solution)/shard_map/reduce_sum | solution.py:35
  45.9 0.2 copy-done.1
  46.1 1.0 fusion.1
  47.1 0.2 copy-done.9
  47.3 1.3 convolution_convert_fusion
  48.6 1.3 convolution_convert_fusion.1
  50.0 0.5 copy.33
  50.6 0.5 broadcast.255
  51.1 0.7 reduce.13
  51.9 5.4 %gather_fusion = bf16[64,128,512]{2,1,0:T(8,128)(2,1)} fusion(bf16[8,128,512]{2,1,0:T(8,128)(2,1)S(1)} %bitcast.170, s32[1024]{0:T(1024)S(1)} %pad_clamp_fusion.1), kind=kCustom, calls=%fused_computation | custom fusion | bytes 16777472 | tf_op jit(solution)/shard_map/gather | solution.py:153
  57.3 32.7 %all-to-all-done = bf16[16,4,64,256]{3,2,1,0:T(8,128)(2,1)} async-done(((bf16[16,4,64,256]{3,2,1,0:T(8,128)(2,1)}), bf16[16,4,64,256]{3,2,1,0:T(8,128)(2,1)}, u32[]{:S(2)}, u32[]{:S(2)}) %all-to-all-start) | async-done | bytes 2097184 | tf_op jit(solution)/shard_map/all_to_all | solution.py:159
  89.9 4.5 %multiply_reduce_fusion.1 = (f32[64,64]{1,0:T(8,128)S(1)}, f32[64,64,128]{2,1,0:T(8,128)S(1)}) fusion(bf16[64,64,256]{2,1,0:T(8,128)(2,1)} %bitcast.41, bf16[64,128,512]{2,1,0:T(8,128)(2,1)} %gather_fusion), kind=kOutput, calls=%fused_computation.26 | convolution fusion | flops 269479936 | bytes 8404992 | tf_op jit(solution)/shard_map/gqhd,grhd->ghqr/dot_general | solution.py:61
  94.4 1.3 fusion.19
  95.8 0.7 reshape.672
  96.5 6.7 %all-to-all-start.2 = ((f32[16,1,512]{2,1,0:T(1,128)}), f32[16,1,512]{2,1,0:T(1,128)S(1)}, u32[]{:S(2)}, u32[]{:S(2)}) async-start(f32[16,1,512]{2,1,0:T(1,128)} %reshape.672), calls=%async_computation.2 | async-start | bytes 65536 | tf_op jit(solution)/shard_map/all_to_all | solution.py:17
  103.2 4.8 %fusion.15 = bf16[64,256,64]{1,2,0:T(8,128)(2,1)} fusion(bf16[64,128,512]{2,1,0:T(8,128)(2,1)} %gather_fusion, f32[64,64,128]{2,1,0:T(8,128)S(1)} %get-tuple-element.48, f32[64,64]{1,0:T(8,128)S(1)} %get-tuple-element.47), kind=kOutput, calls=%fused_computation.27 | convolution fusion | flops 271056896 | bytes 8404992 | tf_op jit(solution)/shard_map/ghqr,grhd->gqhd/dot_general | solution.py:68
  108.0 1.5 all-to-all-done.2
  109.5 5.9 %all-to-all-start.3 = ((bf16[16,4,64,256]{3,2,1,0:T(8,128)(2,1)}), bf16[16,4,64,256]{3,2,1,0:T(8,128)(2,1)S(1)}, u32[]{:S(2)}, u32[]{:S(2)}) async-start(bf16[16,4,64,256]{3,2,1,0:T(8,128)(2,1)} %bitcast.171), calls=%async_computation.3 | async-start | bytes 4194304 | tf_op jit(solution)/shard_map/all_to_all | solution.py:169
  115.4 2.6 %fusion.34 = f32[512,128]{1,0:T(8,128)S(1)} fusion(bf16[2048,128]{1,0:T(8,128)(2,1)} %param.20, bf16[512,2048]{1,0:T(8,128)(2,1)} %param.16, f32[2048]{0:T(1024)S(1)} %copy-done.12, f32[512]{0:T(512)S(1)} %add_rsqrt_fusion.1), kind=kOutput, calls=%fused_computation.74 | convolution fusion | flops 272629760 | bytes 2893824 | tf_op jit(solution)/shard_map/dot_general | solution.py:196
  118.1 0.8 bitcast_convert_fusion.31
  118.9 1.1 fusion.105
  120.0 14.2 %all-reduce.1 = (f32[512]{0:T(512)S(1)}, f32[512]{0:T(512)S(1)}) all-reduce(f32[512]{0:T(512)S(1)} %bitcast.188, f32[512]{0:T(512)S(1)} %bitcast.187), channel_id=1, replica_groups=mesh['grp'=2,'st'=16,'tp'=8] {'tp'}, use_global_device_ids=true, to_apply=%region_4.5 | all-reduce | flops 1024 | bytes 8192 | tf_op jit(solution)/shard_map/psum | solution.py:202
  134.2 0.2 multiply_convert_fusion
  134.5 0.6 broadcast.259
  135.1 1.5 reduce.14
  136.7 0.6 gather_fusion.3
  137.2 0.6 gather_fusion.1
  137.9 0.9 copy.30
  138.8 23.8 %all-to-all-done.3 = bf16[16,4,64,256]{3,2,1,0:T(8,128)(2,1)S(1)} async-done(((bf16[16,4,64,256]{3,2,1,0:T(8,128)(2,1)}), bf16[16,4,64,256]{3,2,1,0:T(8,128)(2,1)S(1)}, u32[]{:S(2)}, u32[]{:S(2)}) %all-to-all-start.3) | async-done | bytes 2097184 | tf_op jit(solution)/shard_map/all_to_all | solution.py:169
  162.6 1.6 gather_fusion.2
  164.2 2.3 %fusion.31 = f32[8,64,1,256]{3,2,1,0:T(1,128)S(1)} fusion(bf16[8,4,64,1]{1,3,2,0:T(2,128)(2,1)} %copy.30, bf16[8,4,64,256]{3,2,1,0:T(8,128)(2,1)} %bitcast.176), kind=kOutput, calls=%fused_computation.42 | convolution fusion | flops 1048576 | bytes 1576960 | tf_op jit(solution)/shard_map/bphq,bpqhd->bqhd/dot_general | solution.py:79
  166.5 0.1 fusion.36
  166.7 0.7 fusion.109
  167.4 0.1 copy-done.3
  167.5 0.7 add_convert_fusion
  168.3 54.5 %all_to_all.29 = bf16[8,64,2048]{2,1,0:T(8,128)(2,1)S(1)} all-to-all(bf16[8,64,2048]{2,1,0:T(8,128)(2,1)S(1)} %bitcast.172), channel_id=1, replica_groups=mesh['grp'=2,'st'=16,'tp'=8] {'tp'}, dimensions={0} | all-to-all | bytes 4194304 | tf_op jit(solution)/shard_map/all_to_all | solution.py:29
  222.8 1.1 reduce_sum.95
  (44 shorter events, 0.6 us)
Async XLA Ops:
  0.0 166.7 %copy-start = (bf16[256,2048]{1,0:T(8,128)(2,1)S(1)}, bf16[256,2048]{1,0:T(8,128)(2,1)}, u32[]{:S(2)}) copy-start(bf16[256,2048]{1,0:T(8,128)(2,1)} %param.30) | copy-start | bytes 3145732
  2.6 32.5 %all-to-all-start.1 = ((s32[16,1,4]{2,1,0:T(1,128)}), s32[16,1,4]{2,1,0:T(1,128)S(1)}, u32[]{:S(2)}, u32[]{:S(2)}) async-start(s32[16,1,4]{2,1,0:T(1,128)} %bitcast.45), calls=%async_computation.1 | async-start | bytes 16384 | tf_op jit(solution)/shard_map/all_to_all | solution.py:137
  35.1 10.8 %copy-start.6 = (f32[2048]{0:T(1024)S(1)}, f32[2048]{0:T(1024)}, u32[]{:S(2)}) copy-start(f32[2048]{0:T(1024)} %param.26) | copy-start | bytes 24580
  35.1 54.8 %all-to-all-start = ((bf16[16,4,64,256]{3,2,1,0:T(8,128)(2,1)}), bf16[16,4,64,256]{3,2,1,0:T(8,128)(2,1)}, u32[]{:S(2)}, u32[]{:S(2)}) async-start(bf16[16,4,64,256]{3,2,1,0:T(8,128)(2,1)} %bitcast.40), calls=%async_computation | async-start | bytes 4194304 | tf_op jit(solution)/shard_map/all_to_all | solution.py:159
  42.6 3.4 %copy-start.1 = (bf16[8,128,2048]{2,1,0:T(8,128)(2,1)S(1)}, bf16[8,128,2048]{2,1,0:T(8,128)(2,1)}, u32[]{:S(2)}) copy-start(bf16[8,128,2048]{2,1,0:T(8,128)(2,1)} %param.17) | copy-start | bytes 12582916
  46.1 1.2 copy-start.9
  47.3 1.3 copy-start.10
  96.5 13.0 %all-to-all-start.2 = ((f32[16,1,512]{2,1,0:T(1,128)}), f32[16,1,512]{2,1,0:T(1,128)S(1)}, u32[]{:S(2)}, u32[]{:S(2)}) async-start(f32[16,1,512]{2,1,0:T(1,128)} %reshape.672), calls=%async_computation.2 | async-start | bytes 65536 | tf_op jit(solution)/shard_map/all_to_all | solution.py:17
  108.0 7.4 %copy-start.5 = (bf16[31,128]{1,0:T(8,128)(2,1)S(1)}, bf16[31,128]{1,0:T(8,128)(2,1)}, u32[]{:S(2)}) copy-start(bf16[31,128]{1,0:T(8,128)(2,1)} %param.22) | copy-start | bytes 23812
  108.0 7.5 %copy-start.12 = (f32[2048]{0:T(1024)S(1)}, f32[2048]{0:T(1024)}, u32[]{:S(2)}) copy-start(f32[2048]{0:T(1024)} %param.19) | copy-start | bytes 24580
  109.5 8.6 %copy-start.4 = (f32[16,1,512]{2,1,0:T(1,128)}, f32[16,1,512]{2,1,0:T(1,128)S(1)}, u32[]{:S(2)}) copy-start(f32[16,1,512]{2,1,0:T(1,128)S(1)} %all-to-all-done.2) | copy-start | bytes 98308
  109.5 53.1 %all-to-all-start.3 = ((bf16[16,4,64,256]{3,2,1,0:T(8,128)(2,1)}), bf16[16,4,64,256]{3,2,1,0:T(8,128)(2,1)S(1)}, u32[]{:S(2)}, u32[]{:S(2)}) async-start(bf16[16,4,64,256]{3,2,1,0:T(8,128)(2,1)} %bitcast.171), calls=%async_computation.3 | async-start | bytes 4194304 | tf_op jit(solution)/shard_map/all_to_all | solution.py:169
  115.4 2.7 %copy-start.2 = (bf16[512,2048]{1,0:T(8,128)(2,1)S(1)}, bf16[512,2048]{1,0:T(8,128)(2,1)}, u32[]{:S(2)}) copy-start(bf16[512,2048]{1,0:T(8,128)(2,1)} %param.16) | copy-start | bytes 6291460
  115.4 2.7 %copy-start.11 = (bf16[2048,128]{1,0:T(8,128)(2,1)S(1)}, bf16[2048,128]{1,0:T(8,128)(2,1)}, u32[]{:S(2)}) copy-start(bf16[2048,128]{1,0:T(8,128)(2,1)} %param.21) | copy-start | bytes 1572868
  118.1 16.2 %copy-start.8 = (f32[128]{0:T(128)S(1)}, f32[128]{0:T(128)}, u32[]{:S(2)}) copy-start(f32[128]{0:T(128)} %param.23) | copy-start | bytes 1540
  166.5 1.0 copy-start.3
  166.5 1.0 copy-start.7
where the time goes:
time: 228 us; the launch traced here: 224 us
  blocking collectives  68.8 us (30%)
  waiting for transfers between devices  57.9 us (25%)
  starting transfers between devices  41.6 us (18%)
  matrix products  21.6 us (9%)
  local copies, waits for them, and re-layouts  20.8 us (9%)
  other arithmetic  12.8 us (6%)
    all_to_all x1, blocking collectives, sent_and_summed(): pieces = lax.all_to_all(cut_along(x, dim, size), axis, 0, 0, tiled=True)  54.5 us
    all_to_all x1, waiting for transfers between devices, local(): lax.all_to_all(slot_queries.reshape(owners, capacity, block_len, head_wid...  32.7 us
    all_to_all x1, waiting for transfers between devices, local(): lax.all_to_all(answer_out.reshape(owners, capacity, block_len, head_width...  23.8 us
    all_to_all x1, starting transfers between devices, local(): lax.all_to_all(slot_ids, 'st', split_axis=0, concat_axis=0, tiled=True)  21.5 us
    psum x1, blocking collectives, local(): lax.psum((jnp.sum(conv_rows, axis=1), jnp.sum(conv_rows * conv_rows, axis...  14.2 us
    all_to_all x1, starting transfers between devices, local(): lax.all_to_all(slot_queries.reshape(owners, capacity, block_len, head_wid...  7.51 us
    all_to_all x1, starting transfers between devices, side_by_side(): lax.all_to_all(both, axis, split_axis=split_dim, concat_axis=concat_dim,...  6.72 us
    all_to_all x1, starting transfers between devices, local(): lax.all_to_all(answer_out.reshape(owners, capacity, block_len, head_width...  5.88 us
  transfers between devices with their start and end apart: 4, of which 3 were waited for; matrix products, arithmetic and copies ran while one was open for 17% of the time, Pallas kernels for 0%

commit v1 on v0

v1 whole, which is shorter than its diff:
```python
import functools

import jax
import jax.numpy as jnp
from jax import lax
from jax.experimental import pallas as pl
from jax.experimental.pallas import tpu as pltpu
from jax.sharding import PartitionSpec as P

CA = 1024
HD = 256
SEQ_LEN = 128
CORES = 2
LANES = 128
EPS = 1e-06
EMPTY = -1e30
MESH = pl.DeviceIdType.MESH
F32 = jnp.float32
BF16 = jnp.bfloat16


def remote(src, dst, send_sem, recv_sem, **target):
    return pltpu.make_async_remote_copy(
        src_ref=src, dst_ref=dst, send_sem=send_sem, recv_sem=recv_sem,
        device_id=target, device_id_type=MESH,
    )


def place_of(distance, n):
    half = n // 2
    return jnp.where(distance >= half, 2 * (distance - half), 2 * (half - distance) - 1)


def order_of(n):
    half = n // 2
    order = [half]
    for j in range(1, half):
        order += [half - j, half + j]
    return order + [0]


def normed_rows(dst, src, gain, rows, step=16):
    @pl.loop(0, rows // step)
    def _(i):
        at = pl.ds(pl.multiple_of(i * step, step), step)
        x = src[at, :].astype(F32)
        inv = lax.rsqrt(jnp.mean(x * x, axis=-1, keepdims=True) + EPS)
        dst[at, :] = (x * inv * gain[...]).astype(BF16)


def serve_kernel(
    n_st, n_tp, slots, blocks, per_block,
    tok_hbm, store_hbm, wq_hbm, wk_hbm, wv_hbm, qgain, pgain, table,
    acc, stats,
    tok, store, wq, wk, wv, xn, *rest,
):
    ring = n_st // CORES
    qall = rest[:ring]
    kall, vall, outs, ml, tabv, tabs, load_sem, q_send, q_recv, kv_send, kv_recv, t_send, t_recv, s_sem = rest[ring:]
    me = lax.axis_index("st")
    x_me = lax.axis_index("tp")
    core = lax.rem(me, CORES)
    y_me = me // CORES
    partner = me + 1 - 2 * core

    def chip(d):
        return lax.rem(me + CORES * d, n_st)

    right, left = chip(1), chip(ring - 1)
    groups = tok_hbm.shape[0] // 128
    passages = store_hbm.shape[0]
    half = ring // 2
    per_group = blocks // groups

    loads = []

    def load(src, dst):
        copy = pltpu.make_async_copy(src, dst, load_sem.at[len(loads)])
        copy.start()
        loads.append(copy)
        return copy

    wq_load = load(wq_hbm, wq)
    tok_loads = [load(tok_hbm.at[pl.ds(g * 128, 128)], tok.at[pl.ds(g * 128, 128)]) for g in range(groups)]
    wk_load = load(wk_hbm, wk)
    wv_load = load(wv_hbm, wv)
    store_loads = [load(store_hbm.at[p], store.at[p]) for p in range(passages)]

    barrier = pltpu.get_barrier_semaphore()
    for d in range(1, ring):
        pl.semaphore_signal(barrier, inc=1, device_id={"st": chip(d)}, device_id_type=MESH)
    pl.semaphore_signal(barrier, inc=1, device_id={"st": partner}, device_id_type=MESH)

    outs[slots] = jnp.zeros(outs.shape[1:], outs.dtype)
    ml[slots, 0:1] = jnp.full((1, LANES), EMPTY, F32)
    ml[slots, 1:2] = jnp.zeros((1, LANES), F32)

    sends = []

    def send(copy):
        copy.start()
        sends.append(copy)

    def part(rel, g):
        return qall[rel].at[pl.ds(per_group * g, per_group)]

    tok_loads[0].wait()
    normed_rows(xn, tok.at[pl.ds(0, 128)], qgain, 128)
    wq_load.wait()
    for g in range(groups):
        if g > 0:
            tok_loads[g].wait()
            normed_rows(xn, tok.at[pl.ds(g * 128, 128)], qgain, 128)
        q = jnp.dot(xn[...], wq[...], preferred_element_type=F32).astype(BF16)
        for i in range(per_group):
            qall[0][per_group * g + i] = q[i * (128 // per_group) : (i + 1) * (128 // per_group)]
        if g == 0:
            pl.semaphore_wait(barrier, ring)
            for d in range(1, ring):
                send(remote(table.at[lax.rem(y_me + d, ring)], tabv.at[ring - d], t_send.at[d - 1],
                            t_recv.at[ring - d - 1], st=chip(d)))
        send(remote(part(0, g), part(ring - 1, g), q_send.at[0, g], q_recv.at[0, g], st=right))
        send(remote(part(0, g), part(1, g), q_send.at[1, g], q_recv.at[1, g], st=left))

    own_table = pltpu.make_async_copy(table.at[y_me], tabv.at[0], s_sem.at[1])
    own_table.start()

    def event(e):
        last = (half - 1) * groups
        if e < last:
            hop, g = e // groups + 1, e % groups
            for side in range(2):
                rel = ring - hop if side == 0 else hop
                here = part(rel, g)
                remote(here, here, q_send.at[side, e], q_recv.at[side, e], st=right).wait_recv()
                if hop < half - 1:
                    nxt = e + groups
                elif side == 0 and g < groups // 2:
                    nxt = last + g
                elif side == 1 and g >= groups // 2:
                    nxt = last + g - groups // 2
                else:
                    continue
                there = part(rel - 1 if side == 0 else rel + 1, g)
                send(remote(here, there, q_send.at[side, nxt], q_recv.at[side, nxt],
                            st=right if side == 0 else left))
        else:
            for side in range(2):
                here = part(half, e - last + side * (groups // 2))
                remote(here, here, q_send.at[side, 0], q_recv.at[side, e], st=right).wait_recv()

    def keys_values(p):
        store_loads[p].wait()
        normed_rows(xn, store.at[p], pgain, 128)
        if p == 0:
            wk_load.wait()
            wv_load.wait()
        at = core * passages + p
        kall[at] = jnp.dot(xn[...], wk[...], preferred_element_type=F32).astype(BF16)
        v = jnp.dot(xn[...], wv[...], preferred_element_type=F32)
        vall[at] = jnp.concatenate([v[:, :LANES].T, v[:, LANES:].T], axis=1).astype(BF16)
        send(remote(kall.at[at], kall.at[at], kv_send.at[0, p], kv_recv.at[0, p], st=partner))
        send(remote(vall.at[at], vall.at[at], kv_send.at[1, p], kv_recv.at[1, p], st=partner))

    low_half = lax.broadcasted_iota(jnp.int32, (LANES, LANES), 1) < LANES // 2

    def attend(rel):
        for k in range(slots):
            q = qall[rel][tabs[rel, 0, k]]
            p = tabs[rel, 0, slots + k]
            s = lax.dot_general(
                kall[p], jnp.concatenate([q, q], axis=0), (((1,), (1,)), ((), ())), preferred_element_type=F32
            ) * HD ** (-0.5)
            top = jnp.max(s, axis=0, keepdims=True)
            e = jnp.exp(s - top)
            ml[k, 0:1] = top
            ml[k, 1:2] = jnp.sum(e, axis=0, keepdims=True)
            w = jnp.concatenate([jnp.where(low_half, e, 0.0), jnp.where(low_half, 0.0, e)], axis=0).astype(BF16)
            outs[k] = jnp.dot(vall[p], w, preferred_element_type=F32).astype(BF16)

        @pl.loop(0, blocks)
        def _(distance):
            b = lax.rem(x_me + distance, blocks)
            at = [tabs[rel, 0, 2 * slots + b * per_block + j] for j in range(per_block)]
            mls = [ml[i] for i in at]
            best = functools.reduce(jnp.maximum, [a[0:1] for a in mls])
            scale = [jnp.exp(a[0:1] - best) for a in mls]
            total = sum(f * a[1:2] for f, a in zip(scale, mls))
            num = sum(f * outs[i].astype(F32) for f, i in zip(scale, at))
            place = place_of(distance, n_tp)
            acc[rel, place] = num.astype(BF16)
            stats[rel, place, 0:1] = best
            stats[rel, place, 1:2] = total

    def all_here():
        for p in range(passages):
            other = (1 - core) * passages + p
            for i, ref in enumerate((kall, vall)):
                remote(ref.at[other], ref.at[other], kv_send.at[i, p], kv_recv.at[i, p], st=partner).wait_recv()
        own_table.wait()
        for d in range(1, ring):
            here = tabv.at[d]
            remote(here, here, t_send.at[d - 1], t_recv.at[d - 1], st=partner).wait_recv()
        to_scalar = pltpu.make_async_copy(tabv, tabs, s_sem.at[0])
        to_scalar.start()
        to_scalar.wait()

    events = (half - 1) * groups + groups // 2
    done = 0
    for p in range(passages):
        keys_values(p)
        if p >= 1:
            event(done)
            done += 1
    all_here()
    turns = [0]
    for hop in range(1, half):
        turns += [ring - hop, hop]
    turns += [half]
    for rel in turns:
        hop = min(rel, ring - rel)
        need = min(hop * groups, events) if hop < half else events
        while done < need:
            event(done)
            done += 1
        attend(rel)
        if done < events:
            event(done)
            done += 1
    for copy in sends:
        copy.wait_send()


def serve(tokens, store, query_proj, key_proj, value_proj, query_gain, passage_gain, table, slots, blocks, per_block):
    n_st, n_tp = lax.axis_size("st"), lax.axis_size("tp")
    ring = n_st // CORES
    rows, width = tokens.shape
    passages, prows, _ = store.shape
    groups = rows // 128
    block_len = rows // blocks
    assert prows == 128 and query_proj.shape[1] == HD and block_len * 2 == LANES and blocks == n_tp
    events = (ring // 2 - 1) * groups + groups // 2
    hbm = pl.BlockSpec(memory_space=pl.ANY)
    vmem = pl.BlockSpec(memory_space=pltpu.VMEM)
    return pl.pallas_call(
        functools.partial(serve_kernel, n_st, n_tp, slots, blocks, per_block),
        out_shape=(
            jax.ShapeDtypeStruct((ring, blocks, LANES, LANES), BF16),
            jax.ShapeDtypeStruct((ring, blocks, 2, LANES), F32),
        ),
        in_specs=[hbm] * 5 + [vmem] * 3,
        out_specs=(vmem, vmem),
        scratch_shapes=[
            pltpu.VMEM((rows, width), BF16),
            pltpu.VMEM(store.shape, BF16),
            pltpu.VMEM(query_proj.shape, BF16),
            pltpu.VMEM(key_proj.shape, BF16),
            pltpu.VMEM(value_proj.shape, BF16),
            pltpu.VMEM((128, width), BF16),
            *[pltpu.VMEM((blocks, block_len, HD), BF16) for _ in range(ring)],
            pltpu.VMEM((CORES * passages, prows, HD), BF16),
            pltpu.VMEM((CORES * passages, LANES, 2 * prows), BF16),
            pltpu.VMEM((slots + 1, LANES, LANES), BF16),
            pltpu.VMEM((slots + 1, 2, LANES), F32),
            pltpu.VMEM(table.shape, jnp.int32),
            pltpu.SMEM(table.shape, jnp.int32),
            pltpu.SemaphoreType.DMA((3 + groups + passages,)),
            pltpu.SemaphoreType.DMA((2, events)),
            pltpu.SemaphoreType.DMA((2, events)),
            pltpu.SemaphoreType.DMA((2, passages)),
            pltpu.SemaphoreType.DMA((2, passages)),
            pltpu.SemaphoreType.DMA((ring - 1,)),
            pltpu.SemaphoreType.DMA((ring - 1,)),
            pltpu.SemaphoreType.DMA((2,)),
        ],
        compiler_params=pltpu.CompilerParams(
            collective_id=0, has_side_effects=True, vmem_limit_bytes=50 * 2**20
        ),
        name="serve",
    )(tokens, store, query_proj, key_proj, value_proj, query_gain, passage_gain, table)


def merged(a, b):
    best = jnp.maximum(a[1], b[1])
    fa, fb = jnp.exp(a[1] - best), jnp.exp(b[1] - best)
    return fa * a[0] + fb * b[0], best, fa * a[2] + fb * b[2]


def blend_kernel(
    n_st, n_tp,
    acc, stats, conv, sums, cgain, mix, attn, blend,
    out,
    ycw, yccw, scw, sccw, xa, xcw, xccw, act, allsums,
    y_send, y_recv, x_send, x_recv, c_send, c_recv,
):
    me = lax.axis_index("st")
    x_me = lax.axis_index("tp")
    ring = n_st // CORES
    half = ring // 2
    xhalf = n_tp // 2
    right, left = lax.rem(me + CORES, n_st), lax.rem(me + n_st - CORES, n_st)
    east, west = lax.rem(x_me + 1, n_tp), lax.rem(x_me + n_tp - 1, n_tp)
    blocks, block_len, width = xa.shape[0] * n_tp, xa.shape[1], xa.shape[2]
    wide = width // 2

    barrier = pltpu.get_barrier_semaphore()
    for who in (right, left):
        pl.semaphore_signal(barrier, inc=1, device_id={"st": who}, device_id_type=MESH)
    for d in range(1, n_tp):
        pl.semaphore_signal(barrier, inc=1, device_id={"tp": lax.rem(x_me + d, n_tp)}, device_id_type=MESH)
    pl.semaphore_wait(barrier, n_tp + 1)

    sends = []

    def send(copy):
        copy.start()
        sends.append(copy)

    for d in range(1, n_tp):
        send(remote(sums, allsums.at[n_tp - d], c_send.at[d - 1], c_recv.at[n_tp - d - 1],
                    tp=lax.rem(x_me + d, n_tp)))

    places = order_of(n_tp)
    chunks = [[0]] + [[2 * j - 1, 2 * j] for j in range(1, xhalf)] + [[n_tp - 1]]
    start_cw = {}
    for c, chunk in enumerate(chunks):
        for i, p in enumerate(chunk):
            start_cw[p] = half if (i == 0 and c < len(chunks) - 1) else half - 1

    sides = (
        (ycw, scw, right, lambda d: d),
        (yccw, sccw, left, lambda d: ring - d),
    )

    def start_of(side, p):
        return start_cw[p] if side == 0 else 2 * half - 1 - start_cw[p]

    def y_send_out(side, p, d, num, stat):
        data, st_, who, _ = sides[side]
        send(remote(num, data.at[p, d - 1], y_send.at[side, p, d - 1, 0], y_recv.at[side, p, d - 1, 0], st=who))
        send(remote(stat, st_.at[p, d - 1], y_send.at[side, p, d - 1, 1], y_recv.at[side, p, d - 1, 1], st=who))

    def y_arrived(side, p, d):
        data, st_, _, _ = sides[side]
        for i, ref in enumerate((data.at[p, d], st_.at[p, d])):
            remote(ref, ref, y_send.at[side, p, d, i], y_recv.at[side, p, d, i], st=right).wait_recv()
        return data[p, d].astype(F32), st_[p, d, 0:1], st_[p, d, 1:2]

    def own(rel, p):
        return acc[rel, p].astype(F32), stats[rel, p, 0:1], stats[rel, p, 1:2]

    def y_start(c, u):
        for p in chunks[c]:
            for side in range(2):
                d = start_of(side, p)
                if d == half - u:
                    rel = sides[side][3](d)
                    y_send_out(side, p, d, acc.at[rel, p], stats.at[rel, p])

    def y_stage(c, u):
        d = half - u
        for p in chunks[c]:
            for side in range(2):
                if d < start_of(side, p):
                    data, st_, _, rel = sides[side]
                    num, best, total = merged(y_arrived(side, p, d), own(rel(d), p))
                    data[p, d] = num.astype(BF16)
                    st_[p, d, 0:1] = best
                    st_[p, d, 1:2] = total
                    y_send_out(side, p, d, data.at[p, d], st_.at[p, d])

    def y_home(p):
        num, best, total = merged(merged(y_arrived(0, p, 0), own(0, p)), y_arrived(1, p, 0))
        t = (num / total).T.astype(BF16)
        return jnp.concatenate([t[:block_len], t[block_len:]], axis=1)

    def activations():
        for d in range(1, n_tp):
            here = allsums.at[d]
            remote(here, here, c_send.at[d - 1], c_recv.at[d - 1], tp=east).wait_recv()
        total = sums[...]
        for d in range(1, n_tp):
            total = total + allsums[d]
        groups = total.shape[0] // 2
        mean = total[:groups] / CA
        var = total[groups:] / CA - mean * mean
        cols = jnp.concatenate([mean, lax.rsqrt(var + EPS)], axis=0).T
        per = 128 // block_len
        for g in range(groups):
            z = conv[pl.ds(g * 128, 128), :]
            z = (z - cols[:, g : g + 1]) * cols[:, groups + g : groups + g + 1] * cgain[...]
            z = (z / (1.0 + jnp.exp(-z))).astype(BF16)
            for i in range(per):
                act[g * per + i] = z[i * block_len : (i + 1) * block_len]

    def x_wait(side, k, h):
        data = (xcw, xccw)[side]
        here = data.at[k, :, pl.ds(h * wide, wide)]
        remote(here, here, x_send.at[side, k, h], x_recv.at[side, k, h], tp=east).wait_recv()

    def x_out(side, k, h, src):
        data = (xcw, xccw)[side]
        send(remote(src, data.at[k - 1, :, pl.ds(h * wide, wide)], x_send.at[side, k - 1, h],
                    x_recv.at[side, k - 1, h], tp=east if side == 0 else west))

    tile = 512

    def project(c):
        chunk = chunks[c]
        k = xhalf - c
        rows_a = jnp.concatenate([y_home(p) for p in chunk], axis=0)
        rows_p = jnp.concatenate([act[lax.rem(x_me + places[p], n_tp)] for p in chunk], axis=0)
        for t in range(width // tile):
            at = pl.ds(t * tile, tile)
            h = t * tile // wide
            first, last = t * tile % wide == 0, (t + 1) * tile % wide == 0
            y = jnp.dot(rows_p, mix[:, at], preferred_element_type=F32) + blend[:, at] * jnp.dot(
                rows_a, attn[:, at], preferred_element_type=F32
            )
            if k == xhalf:
                xa[0, :, at] = y.astype(BF16)
                if last:
                    x_out(h, k, h, xa.at[0, :, pl.ds(h * wide, wide)])
            elif k > 0:
                for side in range(2):
                    data = (xcw, xccw)[side]
                    mine = y[side * block_len : (side + 1) * block_len]
                    if k < xhalf - 1 or h == side:
                        if first:
                            x_wait(side, k, h)
                        mine = mine + data[k, :, at].astype(F32)
                    data[k, :, at] = mine.astype(BF16)
                    if last:
                        x_out(side, k, h, data.at[k, :, pl.ds(h * wide, wide)])
            else:
                for side in range(2):
                    if first:
                        x_wait(side, 0, h)
                y = y + xcw[0, :, at].astype(F32) + xccw[0, :, at].astype(F32)
                out[:, at] = y.astype(BF16)

    n_chunks = len(chunks)
    for turn in range(n_chunks + half):
        for c in range(n_chunks):
            u = turn - c
            if 1 <= u < half:
                y_stage(c, u)
        for c in range(n_chunks):
            if turn == max(c - 1, 0):
                y_start(c, 0)
            if turn == c + 1 - (1 if c > 1 else 0):
                y_start(c, 1)
        if turn == 1:
            activations()
        c = turn - half
        if 0 <= c < n_chunks:
            project(c)
    for copy in sends:
        copy.wait_send()


def blended_rows(acc, stats, conv, sums, channel_gain, mix_out, attn_out, blend_gain):
    n_st, n_tp = lax.axis_size("st"), lax.axis_size("tp")
    ring = n_st // CORES
    half, xhalf = ring // 2, n_tp // 2
    rows, width = conv.shape[0], mix_out.shape[1]
    mine = rows // n_tp
    blocks = acc.shape[1]
    vmem = pl.BlockSpec(memory_space=pltpu.VMEM)
    return pl.pallas_call(
        functools.partial(blend_kernel, n_st, n_tp),
        out_shape=jax.ShapeDtypeStruct((mine, width), BF16),
        in_specs=[vmem] * 8,
        out_specs=vmem,
        scratch_shapes=[
            pltpu.VMEM((blocks, half, LANES, LANES), BF16),
            pltpu.VMEM((blocks, half, LANES, LANES), BF16),
            pltpu.VMEM((blocks, half, 2, LANES), F32),
            pltpu.VMEM((blocks, half, 2, LANES), F32),
            pltpu.VMEM((1, mine, width), BF16),
            pltpu.VMEM((xhalf, mine, width), BF16),
            pltpu.VMEM((xhalf, mine, width), BF16),
            pltpu.VMEM((blocks, mine, conv.shape[1]), BF16),
            pltpu.VMEM((n_tp,) + sums.shape, F32),
            pltpu.SemaphoreType.DMA((2, blocks, half, 2)),
            pltpu.SemaphoreType.DMA((2, blocks, half, 2)),
            pltpu.SemaphoreType.DMA((2, xhalf, 2)),
            pltpu.SemaphoreType.DMA((2, xhalf, 2)),
            pltpu.SemaphoreType.DMA((n_tp - 1,)),
            pltpu.SemaphoreType.DMA((n_tp - 1,)),
        ],
        compiler_params=pltpu.CompilerParams(
            collective_id=1, has_side_effects=True, vmem_limit_bytes=50 * 2**20
        ),
        name="blend",
    )(acc, stats, conv, sums, channel_gain, mix_out, attn_out, blend_gain)


def rms_rows(row_data, gain_vec):
    floats = row_data.astype(F32)
    inv_scale = lax.rsqrt(jnp.mean(floats * floats, axis=-1, keepdims=True) + EPS)
    return (floats * inv_scale * gain_vec).astype(BF16)


def depthwise(gated_rows, conv_taps):
    span_width = conv_taps.shape[0]
    half_span = (span_width - 1) // 2
    seq_length = gated_rows.shape[1]
    padded = jnp.pad(gated_rows.astype(F32), ((0, 0), (half_span, span_width - 1 - half_span), (0, 0)))
    running = jnp.zeros(gated_rows.shape, F32)
    for tap_index in range(span_width):
        running = running + padded[:, tap_index : tap_index + seq_length] * conv_taps[tap_index].astype(F32)
    return running


def request_tables(passage_ids, chips, chip_passages, slots):
    blocks, per_block = passage_ids.shape
    flat = passage_ids.reshape(-1)
    number = jnp.arange(flat.shape[0])
    chip_of = flat // chip_passages
    local_of = flat - chip_of * chip_passages
    earlier = (chip_of[:, None] == chip_of[None, :]) & (number[None, :] < number[:, None])
    rank = jnp.sum(earlier.astype(jnp.int32), axis=1)
    here = jnp.arange(chips)[:, None] == chip_of[None, :]
    taken = here[:, None, :] & (jnp.arange(slots)[None, :, None] == rank[None, None, :])
    block_of = jnp.sum(jnp.where(taken, number // per_block, 0), axis=2)
    passage_of = jnp.sum(jnp.where(taken, local_of, 0), axis=2)
    slot_of = jnp.where(here, rank, slots)
    table = jnp.concatenate([block_of, passage_of, slot_of], axis=1).astype(jnp.int32)
    return jnp.pad(table, ((0, 0), (0, LANES - table.shape[1])))[:, None, :]


def local(
    tokens, store, passage_ids, mix_gain, glu_value, glu_gate, conv_taps, channel_gain, mix_out,
    query_gain, passage_gain, query_proj, key_proj, value_proj, attn_out, blend_gain,
):
    owners = lax.axis_size("st")
    blocks, per_block = passage_ids.shape
    slots = CORES * (2 * blocks * per_block // owners)
    chips = owners // CORES
    table = request_tables(passage_ids, chips, CORES * store.shape[0], slots)
    acc, stats = serve(
        tokens, store, query_proj, key_proj, value_proj, query_gain[None], passage_gain[None], table,
        slots, blocks, per_block,
    )
    rows, channels = tokens.shape[0], glu_value.shape[1]
    mix_input = rms_rows(tokens, mix_gain)
    value_part = jnp.dot(mix_input, glu_value, preferred_element_type=F32)
    gate_part = jnp.dot(mix_input, glu_gate, preferred_element_type=F32)
    gated_rows = (value_part * jax.nn.sigmoid(gate_part)).astype(BF16)
    conv_rows = depthwise(gated_rows.reshape(-1, SEQ_LEN, channels), conv_taps).reshape(rows, channels)
    sums = jnp.concatenate(
        [jnp.sum(conv_rows, axis=1).reshape(-1, 128), jnp.sum(conv_rows * conv_rows, axis=1).reshape(-1, 128)], axis=0
    )
    return blended_rows(
        acc, stats, conv_rows, sums, channel_gain[None], mix_out, attn_out, blend_gain[None]
    )


def solution(mesh):
    in_specs = (
        P(("grp", "st"), None),
        P(("grp", "st"), None, None),
        P(("grp", "st"), None),
        P(),
        P(None, "tp"),
        P(None, "tp"),
        P(None, "tp"),
        P("tp"),
        P("tp", None),
        P(),
        P(),
        P(None, "tp"),
        P(None, "tp"),
        P(None, "tp"),
        P("tp", None),
        P(),
    )
    out_specs = P(("grp", "st", "tp"), None)
    return jax.shard_map(local, mesh=mesh, in_specs=in_specs, out_specs=out_specs, check_vma=False)
```

time: 228 us -> 111 us (0.49); the launches traced: 224 us -> 110 us
  Pallas kernels: 0 us -> 99 us
  blocking collectives: 68.8 us -> 0 us
  waiting for transfers between devices: 57.9 us -> 0 us
  starting transfers between devices: 41.6 us -> 0 us
  local copies, waits for them, and re-layouts: 20.8 us -> 1.63 us
  matrix products: 21.6 us -> 3.12 us
  other arithmetic: 12.8 us -> 5.96 us
    pallas_call x0 -> x2, Pallas kernels: none -> 99 us  [the longest x1 50.3 us: blended_rows(): pl.pallas_call(functools.partial(blend_kernel, n_st, n_tp), out_shape=jax...]
    all_to_all x4 -> x0, waiting for transfers between devices: 57.9 us -> none  [the longest x1 32.7 us: local(): lax.all_to_all(slot_queries.reshape(owners, capacity, block_len, head_wid...]
    all_to_all x1 -> x0, blocking collectives: 54.5 us -> none  [sent_and_summed(): pieces = lax.all_to_all(cut_along(x, dim, size), axis, 0, 0, tiled=True)]
    all_to_all x4 -> x0, starting transfers between devices: 41.6 us -> none  [the longest x1 21.5 us: local(): lax.all_to_all(slot_ids, 'st', split_axis=0, concat_axis=0, tiled=True)]
    dot_general x10 -> x2, matrix products: 21.6 us -> 3.12 us  [the longest x1 2.35 us: local(): value_part = jnp.dot(mix_input, glu_value, preferred_element_type=F32)]
    psum x1 -> x0, blocking collectives: 14.2 us -> none  [local(): lax.psum((jnp.sum(conv_rows, axis=1), jnp.sum(conv_rows * conv_rows, axis...]
    gather x4 -> x0, local copies, waits for them, and re-layouts: 8.12 us -> none  [the longest x1 5.37 us: local(): served = memory[asked.reshape(owners * capacity)]]
    scatter x2 -> x0, local copies, waits for them, and re-layouts: 5.27 us -> none  [the longest x1 4.6 us: local(): slot_queries = jnp.zeros((owners * capacity, block_len, head_width), jnp....]
  transfers between devices with their start and end apart: 4 -> 0, of which waited for: 3 -> 0; matrix products, arithmetic and copies ran while one was open for 17% -> 0% of each run, Pallas kernels for 0% -> 0%
where the time goes in v1:
time: 111 us; the launch traced here: 110 us
  Pallas kernels  99 us (89%)
  other arithmetic  5.96 us (5%)
  matrix products  3.12 us (3%)
  local copies, waits for them, and re-layouts  1.63 us (1%)
    pallas_call x1, Pallas kernels, blended_rows(): pl.pallas_call(functools.partial(blend_kernel, n_st, n_tp), out_shape=jax...  50.3 us
    pallas_call x1, Pallas kernels, serve(): pl.pallas_call(functools.partial(serve_kernel, n_st, n_tp, slots, blocks,...  48.7 us
    dot_general x1, matrix products, local(): value_part = jnp.dot(mix_input, glu_value, preferred_element_type=F32)  2.35 us
    reduce_sum x1, other arithmetic, rms_rows(): jnp.mean(floats * floats, axis=-1, keepdims=True) + EPS  2.23 us

profile of v1, /device:TPU:528, one launch (start us, length us, event | category | flops | bytes accessed | tf_op | source)
XLA Modules:
  0.0 110.0 jit_solution(4007738593272556758)
XLA Ops:
  0.0 0.0 copy-start
  0.0 0.0 copy-start.10
  0.0 0.0 copy-start.12
  0.0 0.0 copy-start.11
  0.0 2.2 %fusion = f32[512]{0:T(512)S(1)} fusion(bf16[512,2048]{1,0:T(8,128)(2,1)} %tok_hbm.1), kind=kLoop, calls=%fused_computation.2 | loop fusion | flops 3145216 | bytes 2099200 | tf_op jit(solution)/shard_map/reduce_sum | solution.py:501
  2.3 0.8 copy.19
  3.0 0.1 reshape.339
  3.1 0.2 convert_reduce_fusion
  3.3 0.4 fusion.71
  3.7 0.1 pad_add_fusion
  3.8 1.0 bitcast_convert_fusion.29
  4.7 1.0 bitcast_convert_fusion.30
  5.7 0.0 copy-done
  5.7 2.3 %fusion.9 = f32[512,128]{1,0:T(8,128)S(1)} fusion(bf16[2048,128]{1,0:T(8,128)(2,1)S(1)} %copy-done, bf16[512,2048]{1,0:T(8,128)(2,1)} %tok_hbm.1, f32[2048]{0:T(1024)} %param.19, f32[512]{0:T(512)S(1)} %add_rsqrt_fusion), kind=kOutput, calls=%fused_computation.41 | convolution fusion | flops 272629760 | bytes 2893824 | tf_op jit(solution)/shard_map/dot_general | solution.py:548
  8.1 0.0 copy-done.10
  8.1 0.0 copy-done.12
  8.1 0.0 copy-done.11
  8.1 0.0 copy-start.1
  8.1 0.0 copy-start.2
  8.2 0.0 copy-start.3
  8.2 0.0 copy-start.7
  8.2 0.0 copy-start.8
  8.2 0.8 bitcast_convert_fusion.31
  9.0 1.1 %fusion.74 = (f32[4,128]{1,0:T(4,128)S(1)}, f32[4,128]{1,0:T(4,128)S(1)}, f32[4,128,128]{2,1,0:T(8,128)S(1)}) fusion(f32[128]{0:T(128)S(1)} %get-tuple-element.45, f32[128]{0:T(128)S(1)} %get-tuple-element.46, f32[128]{0:T(128)S(1)} %get-tuple-element.17, f32[128]{0:T(128)S(1)} %get-tuple-element.18, f32[128]{0:T(128)S(1)} %get-tuple-element.19, ...), kind=kLoop, calls=%fused_computation.156 | loop fusion | flops 4193280 | bytes 544256 | tf_op jit(solution)/shard_map/reduce_sum | solution.py:553
  10.1 0.0 copy-done.1
  10.1 0.0 copy-done.2
  10.1 0.0 copy-done.3
  10.1 0.0 copy-done.7
  10.1 0.0 copy-done.8
  10.2 0.0 copy-start.4
  10.2 0.0 copy-start.5
  10.2 0.0 copy-start.6
  10.2 0.0 copy-start.9
  10.2 48.7 %serve.1 = (bf16[8,8,128,128]{3,2,1,0:T(8,128)(2,1)}, f32[8,8,2,128]{3,2,1,0:T(2,128)S(1)}) custom-call(bf16[512,2048]{1,0:T(8,128)(2,1)} %tok_hbm.1, bf16[8,128,2048]{2,1,0:T(8,128)(2,1)} %store_hbm.1, bf16[2048,256]{1,0:T(8,128)(2,1)S(1)} %copy-done.1, bf16[2048,256]{1,0:T(8,128)(2,1)S(1)} %copy-done.2, bf16[2048,256]{1,0:T(8,128)(2,1)S(1)} %copy-done.3, ...), custom_call_target="tpu_custom_call" | custom-call | tf_op jit(solution)/shard_map/serve/pallas_call | solution.py:245
  59.0 0.0 copy-done.4
  59.0 0.0 copy-done.5
  59.0 0.0 copy-done.6
  59.0 0.0 copy-done.9
  59.0 50.3 %blend.1 = bf16[64,2048]{1,0:T(8,128)(2,1)S(1)} custom-call(bf16[8,8,128,128]{3,2,1,0:T(8,128)(2,1)} %get-tuple-element.7.acc, f32[8,8,2,128]{3,2,1,0:T(2,128)S(1)} %get-tuple-element.8.stats, f32[512,128]{1,0:T(8,128)S(1)} %bitcast.106, f32[8,128]{1,0:T(8,128)S(1)} %pad_maximum_fusion.sums, f32[1,128]{1,0:T(1,128)S(1)} %bitcast.111, ...), custom_call_target="tpu_custom_call" | custom-call | tf_op jit(solution)/shard_map/blend/pallas_call | solution.py:470
  109.3 0.7 copy.21
  (7 shorter events, 0.1 us)
Async XLA Ops:
  0.0 5.7 %copy-start = (bf16[2048,128]{1,0:T(8,128)(2,1)S(1)}, bf16[2048,128]{1,0:T(8,128)(2,1)}, u32[]{:S(2)}) copy-start(bf16[2048,128]{1,0:T(8,128)(2,1)} %param.20) | copy-start | bytes 1572868
  0.0 8.1 %copy-start.10 = (bf16[512,2048]{1,0:T(8,128)(2,1)S(1)}, bf16[512,2048]{1,0:T(8,128)(2,1)}, u32[]{:S(2)}) copy-start(bf16[512,2048]{1,0:T(8,128)(2,1)} %tok_hbm.1) | copy-start | bytes 6291460
  0.0 8.1 %copy-start.12 = (f32[2048]{0:T(1024)S(1)}, f32[2048]{0:T(1024)}, u32[]{:S(2)}) copy-start(f32[2048]{0:T(1024)} %param.19) | copy-start | bytes 24580
  0.0 8.1 %copy-start.11 = (bf16[2048,128]{1,0:T(8,128)(2,1)S(1)}, bf16[2048,128]{1,0:T(8,128)(2,1)}, u32[]{:S(2)}) copy-start(bf16[2048,128]{1,0:T(8,128)(2,1)} %param.21) | copy-start | bytes 1572868
  8.1 2.0 %copy-start.1 = (bf16[2048,256]{1,0:T(8,128)(2,1)S(1)}, bf16[2048,256]{1,0:T(8,128)(2,1)}, u32[]{:S(2)}) copy-start(bf16[2048,256]{1,0:T(8,128)(2,1)} %wq_hbm.1) | copy-start | bytes 3145732
  8.1 2.0 %copy-start.2 = (bf16[2048,256]{1,0:T(8,128)(2,1)S(1)}, bf16[2048,256]{1,0:T(8,128)(2,1)}, u32[]{:S(2)}) copy-start(bf16[2048,256]{1,0:T(8,128)(2,1)} %wk_hbm.1) | copy-start | bytes 3145732
  8.2 2.0 %copy-start.3 = (bf16[2048,256]{1,0:T(8,128)(2,1)S(1)}, bf16[2048,256]{1,0:T(8,128)(2,1)}, u32[]{:S(2)}) copy-start(bf16[2048,256]{1,0:T(8,128)(2,1)} %wv_hbm.1) | copy-start | bytes 3145732
  8.2 2.0 %copy-start.7 = (f32[2048]{0:T(1024)S(1)}, f32[2048]{0:T(1024)}, u32[]{:S(2)}) copy-start(f32[2048]{0:T(1024)} %param.25) | copy-start | bytes 24580
  8.2 2.0 %copy-start.8 = (f32[2048]{0:T(1024)S(1)}, f32[2048]{0:T(1024)}, u32[]{:S(2)}) copy-start(f32[2048]{0:T(1024)} %param.26) | copy-start | bytes 24580
  10.2 48.8 %copy-start.4 = (bf16[256,2048]{1,0:T(8,128)(2,1)S(1)}, bf16[256,2048]{1,0:T(8,128)(2,1)}, u32[]{:S(2)}) copy-start(bf16[256,2048]{1,0:T(8,128)(2,1)} %attn.1) | copy-start | bytes 3145732
  10.2 48.8 %copy-start.5 = (bf16[128,2048]{1,0:T(8,128)(2,1)S(1)}, bf16[128,2048]{1,0:T(8,128)(2,1)}, u32[]{:S(2)}) copy-start(bf16[128,2048]{1,0:T(8,128)(2,1)} %mix.1) | copy-start | bytes 1572868
  10.2 48.8 %copy-start.6 = (f32[2048]{0:T(1024)S(1)}, f32[2048]{0:T(1024)}, u32[]{:S(2)}) copy-start(f32[2048]{0:T(1024)} %param.31) | copy-start | bytes 24580
  10.2 48.8 %copy-start.9 = (f32[128]{0:T(128)S(1)}, f32[128]{0:T(128)}, u32[]{:S(2)}) copy-start(f32[128]{0:T(128)} %param.23) | copy-start | bytes 1540

commit v2 on v0

v2 whole, which is shorter than its diff:
```python
import functools

import jax
import jax.numpy as jnp
from jax import lax
from jax.experimental import pallas as pl
from jax.experimental.pallas import tpu as pltpu
from jax.sharding import PartitionSpec as P

CA = 1024
HD = 256
SEQ_LEN = 128
CORES = 2
LANES = 128
EPS = 1e-06
EMPTY = -1e30
BACKLOG = {5: 9.0, 6: 9.0, 7: 1.2, 8: 0.0, 9: 0.0}
MESH = pl.DeviceIdType.MESH
F32 = jnp.float32
BF16 = jnp.bfloat16


def remote(src, dst, send_sem, recv_sem, **target):
    return pltpu.make_async_remote_copy(
        src_ref=src, dst_ref=dst, send_sem=send_sem, recv_sem=recv_sem,
        device_id=target, device_id_type=MESH,
    )


def place_of(distance, n):
    half = n // 2
    return jnp.where(distance >= half, 2 * (distance - half), 2 * (half - distance) - 1)


def order_of(n):
    half = n // 2
    order = [half]
    for j in range(1, half):
        order += [half - j, half + j]
    return order + [0]


def normed_rows(dst, src, gain, rows, step=16, unroll=2):
    @pl.loop(0, rows // step, unroll=unroll)
    def _(i):
        at = pl.ds(pl.multiple_of(i * step, step), step)
        x = src[at, :].astype(F32)
        inv = lax.rsqrt(jnp.mean(x * x, axis=-1, keepdims=True) + EPS)
        dst[at, :] = (x * inv * gain[...]).astype(BF16)


def merged(a, b):
    best = jnp.maximum(a[1], b[1])
    fa, fb = jnp.exp(a[1] - best), jnp.exp(b[1] - best)
    return fa * a[0] + fb * b[0], best, fa * a[2] + fb * b[2]


class Plan:
    def __init__(self):
        self.steps = {}

    def add(self, name, run, time, rank, after=(), gets=(), sends=()):
        self.steps[name] = (run, time, rank, tuple(after), tuple(gets), tuple(sends))

    def order(self, backlog):
        clock, free, arrival, done, order = 0.0, {}, {}, set(), []
        left = list(self.steps)
        while left:
            best = None
            for name in left:
                _, _, rank, after, gets, sends = self.steps[name]
                if all(a in done for a in after) and all(g in arrival for g in gets):
                    ready = max([clock] + [arrival[g] for g in gets])
                    if rank in backlog:
                        ready = max([ready] + [free.get(link, 0.0) - backlog[rank] for _, link, _, _ in sends])
                    if best is None or (ready, rank) < best[0]:
                        best = ((ready, rank), name)
            (ready, _), name = best
            _, time, _, _, _, sends = self.steps[name]
            clock = ready + time
            for message, link, wire, late in sends:
                free[link] = max(free.get(link, 0.0), clock) + wire
                arrival[message] = free[link] + late
            done.add(name)
            left.remove(name)
            order.append((name, ready, clock))
        return order


def step_plan(k):
    plan = Plan()
    ring, half, groups, xhalf = k.ring, k.half, k.groups, k.xhalf
    hop_late, far_late, q_wire, y_wire, x_wire = 2.3, 0.75, 1.4, 0.72, 1.4
    for g in range(groups):
        plan.add(
            ("q", g), functools.partial(k.queries, g), 0.76, 1, [("q", g - 1)] if g else [],
            sends=[(("q", side, 1, g), ("y", side), q_wire, hop_late) for side in range(2)],
        )
    for hop in range(1, half + 1):
        for g in range(groups):
            for side in range(2):
                if hop == half and (g < groups // 2) != (side == 0):
                    continue
                on = hop + 1 < half or (hop + 1 == half and (g < groups // 2) == (side == 0))
                plan.add(
                    ("hand", side, hop, g), functools.partial(k.hand_on, side, hop, g, on), 0.03, 0,
                    gets=[("q", side, hop, g)],
                    sends=[(("q", side, hop + 1, g), ("y", side), q_wire, hop_late)] if on else [],
                )
    pairs = list(range(0, k.passages, 2))
    for p in pairs:
        plan.add(("norm", p), functools.partial(k.norm_passages, p), 0.75, 20, [("v", p - 2)] if p else [("q", groups - 1)])
        plan.add(("k", p), functools.partial(k.keys, p), 0.5, 20, [("norm", p)])
        plan.add(("v", p), functools.partial(k.values, p), 0.65, 20, [("k", p)], sends=[(("kv", p), ("core",), 0.4, 1.0)])
    plan.add(("here",), k.all_here, 0.65, 21, [("v", p) for p in pairs], gets=[("kv", p) for p in pairs])
    for rel in range(ring):
        hop = min(rel, ring - rel)
        if hop == half:
            hands = [("hand", 0 if g < groups // 2 else 1, hop, g) for g in range(groups)]
        elif hop:
            hands = [("hand", 1 if rel < half else 0, hop, g) for g in range(groups)]
        else:
            hands = []
        plan.add(("slots", rel), functools.partial(k.attend, rel), 0.6, 19 - hop, [("here",)] + hands)
        plan.add(("attend", rel), functools.partial(k.join, rel), 0.4, 1, [("slots", rel)])
    for c, chunk in enumerate(k.chunks):
        for p in chunk:
            joined = k.join_side(p)
            if joined is not None:
                plan.add(
                    ("join", p), functools.partial(k.join_late, p), 0.03, 5 + c, [("attend", half)],
                    sends=[(("join", p), ("y", joined), y_wire * (half - k.join_hop(p)),
                            hop_late + far_late * (half - k.join_hop(p) - 1))],
                )
            for side in range(2):
                far = k.start_of(side, p)
                for d in range(far, 0, -1):
                    rel = d if side == 0 else ring - d
                    gets = [] if d == far else [("y", side, p, d)]
                    if joined == side and d == k.join_hop(p):
                        gets = gets + [("join", p)]
                    plan.add(
                        ("y", side, p, d),
                        functools.partial(k.y_start if d == far else k.y_stage, side, p, d), 0.03 if d == far else 0.1,
                        5 + c, [("attend", rel)], gets=gets,
                        sends=[(("y", side, p, d - 1), ("y", side), y_wire, hop_late)],
                    )
    for g in range(groups):
        plan.add(("glu", g), functools.partial(k.glu, g), 0.95, 30, [("q", groups - 1)])
        plan.add(("conv", g), functools.partial(k.convolve, g), 0.25, 29, [("glu", g)])
    plan.add(("sums",), k.send_sums, 0.1, 3, [("conv", g) for g in range(groups)],
             sends=[(("sums",), ("x", 2), 0.5, 5.0)])
    plan.add(("act",), k.activations, 0.4, 4, gets=[("sums",)])
    for c, chunk in enumerate(k.chunks):
        gets = [("y", side, p, 0) for p in chunk for side in range(2)]
        gets += [("join", p) for p in chunk if k.join_side(p) is not None and k.join_hop(p) == 0]
        plan.add(("home", c), functools.partial(k.home, c), 0.3, 4, [("attend", 0)], gets=gets)
        dist = xhalf - c
        for t in range(k.tiles):
            h = t // (k.tiles // 2)
            if dist == xhalf:
                gets, outs = [], [h]
            elif dist == 0:
                gets, outs = [0, 1], []
            else:
                gets = [0, 1] if dist < xhalf - 1 else [h]
                outs = [0, 1]
            plan.add(
                ("project", c, t), functools.partial(k.project, c, t, gets, outs), 0.25, 3, [("home", c), ("act",)],
                gets=[("x", side, dist, t) for side in gets],
                sends=[(("x", side, dist - 1, t), ("x", side), x_wire, hop_late) for side in outs],
            )
    return plan


class Body:
    def __init__(self, n_st, n_tp, slots, blocks, per_block, refs):
        self.__dict__.update(refs)
        self.n_st, self.n_tp, self.slots, self.blocks, self.per_block = n_st, n_tp, slots, blocks, per_block
        self.ring, self.groups = n_st // CORES, self.tok_hbm.shape[0] // 128
        self.half, self.xhalf = self.ring // 2, n_tp // 2
        self.passages = self.store_hbm.shape[0]
        self.per_group = blocks // self.groups
        self.block_len = 128 // self.per_group
        self.width = self.tok_hbm.shape[1]
        self.tile = 512
        self.tiles = self.width // self.tile
        self.me, self.x_me = lax.axis_index("st"), lax.axis_index("tp")
        self.core, self.y_me = lax.rem(self.me, CORES), self.me // CORES
        self.partner = self.me + 1 - 2 * self.core
        self.right, self.left = self.chip(1), self.chip(self.ring - 1)
        self.sends, self.loads = [], []
        self.early = 2
        self.places = order_of(n_tp)
        self.chunks = [[0]] + [[2 * j - 1, 2 * j] for j in range(1, self.xhalf)] + [[n_tp - 1]]
        self.start_cw = {}
        for c, chunk in enumerate(self.chunks):
            for i, p in enumerate(chunk):
                self.start_cw[p] = self.half if (i == 0 and c < len(self.chunks) - 1) else self.half - 1

    def chip(self, d):
        return lax.rem(self.me + CORES * d, self.n_st)

    def column(self, d):
        return lax.rem(self.x_me + d, self.n_tp)

    def send(self, copy):
        copy.start()
        self.sends.append(copy)

    def load(self, src, dst):
        copy = pltpu.make_async_copy(src, dst, self.load_sem.at[len(self.loads)])
        copy.start()
        self.loads.append(copy)
        return copy

    def start_of(self, side, p):
        if self.join_side(p) is not None:
            return self.half - 1
        return self.start_cw[p] if side == 0 else 2 * self.half - 1 - self.start_cw[p]

    def enter(self):
        small = lambda name: self.load(getattr(self, name + "_hbm"), getattr(self, name))
        self.first_loads = [small("qgain"), self.load(self.wq_hbm, self.wq)]
        rows = lambda g: pl.ds(g * 128, 128)
        self.tok_loads = [self.load(self.tok_hbm.at[rows(g)], self.tok.at[rows(g)]) for g in range(self.groups)]
        self.table_load = small("table")
        self.kv_loads = [small("pgain"), self.load(self.wk_hbm, self.wk), self.load(self.wv_hbm, self.wv)]
        self.store_loads = [
            self.load(self.store_hbm.at[p], self.store.at[pl.ds(p * 128, 128)]) for p in range(self.passages)
        ]
        self.glu_loads = [
            small("mgain"), small("taps"), small("cgain"),
            self.load(self.gv_hbm, self.wglu.at[:, pl.ds(0, LANES)]),
            self.load(self.gg_hbm, self.wglu.at[:, pl.ds(LANES, LANES)]),
        ]
        self.out_loads = [small("blend"), self.load(self.attn_hbm, self.attn), self.load(self.mix_hbm, self.mix)]
        barrier = pltpu.get_barrier_semaphore()
        for d in range(1, self.ring):
            pl.semaphore_signal(barrier, inc=1, device_id={"st": self.chip(d)}, device_id_type=MESH)
        pl.semaphore_signal(barrier, inc=1, device_id={"st": self.partner}, device_id_type=MESH)
        for d in range(1, self.n_tp):
            pl.semaphore_signal(barrier, inc=1, device_id={"tp": self.column(d)}, device_id_type=MESH)
        s = self.slots
        self.outs[s] = jnp.zeros(self.outs.shape[1:], BF16)
        self.ml[s, 0:1] = jnp.full((1, LANES), EMPTY, F32)
        self.ml[s, 1:2] = jnp.zeros((1, LANES), F32)
        self.padded[...] = jnp.zeros(self.padded.shape, F32)

    def entered(self):
        self.table_load.wait()
        pl.semaphore_wait(pltpu.get_barrier_semaphore(), self.ring + self.n_tp - 1)
        for d in range(1, self.ring):
            self.send(remote(self.table.at[lax.rem(self.y_me + d, self.ring)], self.tabv.at[self.ring - d],
                             self.t_send.at[d - 1], self.t_recv.at[self.ring - d - 1], st=self.chip(d)))
        self.own_table = pltpu.make_async_copy(self.table.at[self.y_me], self.tabv.at[0], self.s_sem.at[1])
        self.own_table.start()


    def part(self, rel, g):
        return self.qall[rel].at[pl.ds(self.per_group * g, self.per_group)]

    def queries(self, g):
        self.tok_loads[g].wait()
        if g == 0:
            self.first_loads[0].wait()
        normed_rows(self.xn.at[pl.ds(0, 128)], self.tok.at[pl.ds(g * 128, 128)], self.qgain, 128, unroll=4)
        if g == 0:
            self.first_loads[1].wait()
        q = jnp.dot(self.xn[pl.ds(0, 128), :], self.wq[...], preferred_element_type=F32).astype(BF16)
        n = self.block_len
        for i in range(self.per_group):
            self.qall[0][self.per_group * g + i] = q[i * n : (i + 1) * n]
        if g == 0:
            with jax.named_scope("entry"):
                self.entered()
        for side, rel, who in ((0, self.ring - 1, self.right), (1, 1, self.left)):
            self.send(remote(self.part(0, g), self.part(rel, g), self.q_send.at[side, 0, g], self.q_recv.at[side, 0, g],
                             st=who))

    def hand_on(self, side, hop, g, on):
        rel = self.ring - hop if side == 0 else hop
        here = self.part(rel, g)
        remote(here, here, self.q_send.at[side, hop - 1, g], self.q_recv.at[side, hop - 1, g], st=self.right).wait_recv()
        if on:
            there = self.part(rel - 1 if side == 0 else rel + 1, g)
            self.send(remote(here, there, self.q_send.at[side, hop, g], self.q_recv.at[side, hop, g],
                             st=self.right if side == 0 else self.left))


    def norm_passages(self, p):
        for i in range(2):
            self.store_loads[p + i].wait()
        if p == 0:
            for copy in self.kv_loads:
                copy.wait()
        normed_rows(self.xn, self.store.at[pl.ds(p * 128, 256)], self.pgain, 256)

    def share(self, j, ref, at, p):
        self.send(remote(ref.at[at], ref.at[at], self.kv_send.at[j, p], self.kv_recv.at[j, p], st=self.partner))

    def keys(self, p):
        k = jnp.dot(self.xn[...], self.wk[...], preferred_element_type=F32).astype(BF16)
        for i in range(2):
            at = self.core * self.passages + p + i
            self.kall[at] = k[i * 128 : (i + 1) * 128]
            self.share(0, self.kall, at, p + i)

    def values(self, p):
        v = jnp.dot(self.xn[...], self.wv[...], preferred_element_type=F32)
        for i in range(2):
            at = self.core * self.passages + p + i
            w = v[i * 128 : (i + 1) * 128]
            self.vall[at] = jnp.concatenate([w[:, :LANES].T, w[:, LANES:].T], axis=1).astype(BF16)
            self.share(1, self.vall, at, p + i)

    def all_here(self):
        for p in range(self.passages):
            other = (1 - self.core) * self.passages + p
            for j, ref in enumerate((self.kall, self.vall)):
                remote(ref.at[other], ref.at[other], self.kv_send.at[j, p], self.kv_recv.at[j, p],
                       st=self.partner).wait_recv()
        self.own_table.wait()
        for d in range(1, self.ring):
            here = self.tabv.at[d]
            remote(here, here, self.t_send.at[d - 1], self.t_recv.at[d - 1], st=self.partner).wait_recv()
        to_scalar = pltpu.make_async_copy(self.tabv, self.tabs, self.s_sem.at[0])
        to_scalar.start()
        to_scalar.wait()


    def attend(self, rel):
        low_half = lax.broadcasted_iota(jnp.int32, (LANES, LANES), 1) < LANES // 2
        slots, tabs, ml, outs = self.slots, self.tabs, self.ml, self.outs
        for k in range(slots):
            q = self.qall[rel][tabs[rel, 0, k]]
            p = tabs[rel, 0, slots + k]
            s = lax.dot_general(
                self.kall[p], jnp.concatenate([q, q], axis=0), (((1,), (1,)), ((), ())), preferred_element_type=F32
            ) * HD ** (-0.5)
            top = jnp.max(s, axis=0, keepdims=True)
            e = jnp.exp(s - top)
            ml[k, 0:1] = top
            ml[k, 1:2] = jnp.sum(e, axis=0, keepdims=True)
            w = jnp.concatenate([jnp.where(low_half, e, 0.0), jnp.where(low_half, 0.0, e)], axis=0).astype(BF16)
            outs[k] = jnp.dot(self.vall[p], w, preferred_element_type=F32).astype(BF16)

    def join(self, rel):
        slots, tabs, ml, outs = self.slots, self.tabs, self.ml, self.outs

        @pl.loop(0, self.blocks)
        def _(distance):
            b = lax.rem(self.x_me + distance, self.blocks)
            at = [tabs[rel, 0, 2 * slots + b * self.per_block + j] for j in range(self.per_block)]
            mls = [ml[i] for i in at]
            best = functools.reduce(jnp.maximum, [a[0:1] for a in mls])
            scale = [jnp.exp(a[0:1] - best) for a in mls]
            total = sum(f * a[1:2] for f, a in zip(scale, mls))
            num = sum(f * outs[i].astype(F32) for f, i in zip(scale, at))
            place = place_of(distance, self.n_tp)
            self.acc[rel, place] = num.astype(BF16)
            self.stats[rel, place, 0:1] = best
            self.stats[rel, place, 1:2] = total


    def y_out(self, side, p, d, num, stat):
        who = self.right if side == 0 else self.left
        for i, (src, dst) in enumerate(((num, self.ydata), (stat, self.ystat))):
            self.send(remote(src, dst.at[side, p, d - 1], self.y_send.at[side, p, d - 1, i],
                             self.y_recv.at[side, p, d - 1, i], st=who))

    def y_start(self, side, p, d):
        rel = d if side == 0 else self.ring - d
        self.y_out(side, p, d, self.acc.at[rel, p], self.stats.at[rel, p])

    def y_arrived(self, side, p, d):
        for i, ref in enumerate((self.ydata, self.ystat)):
            here = ref.at[side, p, d]
            remote(here, here, self.y_send.at[side, p, d, i], self.y_recv.at[side, p, d, i], st=self.right).wait_recv()
        stat = self.ystat.at[side, p, d]
        return self.ydata[side, p, d].astype(F32), stat[0:1], stat[1:2]

    def own(self, rel, p):
        return self.acc[rel, p].astype(F32), self.stats[rel, p, 0:1], self.stats[rel, p, 1:2]

    def y_stage(self, side, p, d):
        so_far = merged(self.y_arrived(side, p, d), self.own(d if side == 0 else self.ring - d, p))
        if self.join_side(p) == side and self.join_hop(p) == d:
            so_far = merged(so_far, self.joined(p))
        num, best, total = so_far
        self.ydata[side, p, d] = num.astype(BF16)
        self.ystat[side, p, d, 0:1] = best
        self.ystat[side, p, d, 1:2] = total
        self.y_out(side, p, d, self.ydata.at[side, p, d], self.ystat.at[side, p, d])

    def join_side(self, p):
        early = [q for chunk in self.chunks[: self.early] for q in chunk]
        return (early.index(p) + 1) % 2 if p in early else None

    def join_hop(self, p):
        return 0 if p == self.chunks[0][0] else 1

    def join_late(self, p):
        side = self.join_side(p)
        hops = self.half - self.join_hop(p)
        who = self.chip(hops if side == 0 else self.ring - hops)
        for i, (src, dst) in enumerate(((self.acc, self.jdata), (self.stats, self.jstat))):
            self.send(remote(src.at[self.half, p], dst.at[p], self.j_send.at[p, i], self.j_recv.at[p, i], st=who))

    def joined(self, p):
        for i, ref in enumerate((self.jdata, self.jstat)):
            here = ref.at[p]
            remote(here, here, self.j_send.at[p, i], self.j_recv.at[p, i], st=self.right).wait_recv()
        stat = self.jstat.at[p]
        return self.jdata[p].astype(F32), stat[0:1], stat[1:2]

    def home(self, c):
        for i, p in enumerate(self.chunks[c]):
            so_far = merged(merged(self.y_arrived(0, p, 0), self.own(0, p)), self.y_arrived(1, p, 0))
            if self.join_side(p) is not None and self.join_hop(p) == 0:
                so_far = merged(so_far, self.joined(p))
            num, best, total = so_far
            t = (num / total).T.astype(BF16)
            n = self.block_len
            self.rows_a[c, pl.ds(i * n, n), :] = jnp.concatenate([t[:n], t[n:]], axis=1)


    def glu(self, g):
        xm = self.xm
        if g == 0:
            for copy in self.glu_loads:
                copy.wait()
        normed_rows(xm, self.tok.at[pl.ds(g * 128, 128)], self.mgain, 128)
        y = jnp.dot(xm[...], self.wglu[...], preferred_element_type=F32)
        gated = y[:, :LANES] * jax.nn.sigmoid(y[:, LANES:])
        self.padded[g, pl.ds(16, 128), :] = gated.astype(BF16).astype(F32)

    def convolve(self, g):
        taps = self.taps[...].astype(F32)
        span = taps.shape[0]
        first = 16 - (span - 1) // 2
        running = jnp.zeros((128, LANES), F32)
        for k in range(span):
            running = running + self.padded[g, pl.ds(first + k, 128), :] * taps[k : k + 1]
        self.conv[g] = running
        turned = running.T
        self.sums[g : g + 1, :] = jnp.sum(turned, axis=0, keepdims=True)
        at = self.groups + g
        self.sums[at : at + 1, :] = jnp.sum(turned * turned, axis=0, keepdims=True)

    def send_sums(self):
        for d in range(1, self.n_tp):
            self.send(remote(self.sums, self.allsums.at[self.n_tp - d], self.c_send.at[d - 1],
                             self.c_recv.at[self.n_tp - d - 1], tp=self.column(d)))

    def activations(self):
        total = self.sums[...]
        for d in range(1, self.n_tp):
            here = self.allsums.at[d]
            remote(here, here, self.c_send.at[d - 1], self.c_recv.at[d - 1], tp=self.column(1)).wait_recv()
            total = total + self.allsums[d]
        groups = self.groups
        mean = total[:groups] / CA
        var = total[groups:] / CA - mean * mean
        cols = jnp.concatenate([mean, lax.rsqrt(var + EPS)], axis=0).T
        n = self.block_len
        for g in range(groups):
            z = (self.conv[g] - cols[:, g : g + 1]) * cols[:, groups + g : groups + g + 1] * self.cgain[...]
            z = (z / (1.0 + jnp.exp(-z))).astype(BF16)
            for i in range(self.per_group):
                self.act[g * self.per_group + i] = z[i * n : (i + 1) * n]


    def project(self, c, t, gets, outs):
        chunk, k, n = self.chunks[c], self.xhalf - c, self.block_len
        at = pl.ds(t * self.tile, self.tile)
        if c == 0 and t == 0:
            for copy in self.out_loads:
                copy.wait()
        rows_p = jnp.concatenate([self.act[self.column(self.places[p])] for p in chunk], axis=0)
        y = jnp.dot(rows_p, self.mix[:, at], preferred_element_type=F32) + self.blend[:, at] * jnp.dot(
            self.rows_a[c, pl.ds(0, n * len(chunk)), :], self.attn[:, at], preferred_element_type=F32
        )
        for side in gets:
            here = self.xdata.at[side, k, t]
            remote(here, here, self.x_send.at[side, k, t], self.x_recv.at[side, k, t], tp=self.column(1)).wait_recv()
        if k == 0:
            y = y + self.xdata[0, k, t].astype(F32) + self.xdata[1, k, t].astype(F32)
            self.out[:, at] = y.astype(BF16)
            return
        for side in outs:
            mine = y if len(chunk) == 1 else y[side * n : (side + 1) * n]
            if side in gets:
                mine = mine + self.xdata[side, k, t].astype(F32)
            slot = self.xdata.at[side, k, t] if k < self.xhalf else self.xfirst.at[t]
            slot[...] = mine.astype(BF16)
            self.send(remote(slot, self.xdata.at[side, k - 1, t], self.x_send.at[side, k - 1, t],
                             self.x_recv.at[side, k - 1, t],
                             tp=self.column(1 if side == 0 else self.n_tp - 1)))


def whole_kernel(names, n_st, n_tp, slots, blocks, per_block, *refs):
    ring = n_st // CORES
    at = names.index("qall")
    found = dict(zip(names[:at] + names[at + 1 :], refs[:at] + refs[at + ring :]))
    found["qall"] = refs[at : at + ring]
    k = Body(n_st, n_tp, slots, blocks, per_block, found)
    plan = step_plan(k)
    with jax.named_scope("enter"):
        k.enter()
    for name, _, _ in plan.order(BACKLOG):
        with jax.named_scope("_".join(str(part) for part in name)):
            plan.steps[name][0]()
    for copy in k.sends:
        copy.wait_send()


def whole(table, slots, blocks, per_block, big, small):
    n_st, n_tp = lax.axis_size("st"), lax.axis_size("tp")
    ring, half, xhalf = n_st // CORES, n_st // CORES // 2, n_tp // 2
    rows, width = big["tok_hbm"].shape
    passages, prows, _ = big["store_hbm"].shape
    groups, block_len, mine = rows // 128, rows // blocks, rows // n_tp
    channels = big["gv_hbm"].shape[1]
    assert prows == 128 and big["wq_hbm"].shape[1] == HD and channels == LANES
    assert block_len * 2 == LANES and blocks == n_tp and passages % 2 == 0
    tiles = width // 512
    dma = pltpu.SemaphoreType.DMA
    scratch = {
        "tok": pltpu.VMEM((rows, width), BF16),
        "store": pltpu.VMEM((passages * prows, width), BF16),
        "wq": pltpu.VMEM((width, HD), BF16),
        "wk": pltpu.VMEM((width, HD), BF16),
        "wv": pltpu.VMEM((width, HD), BF16),
        "wglu": pltpu.VMEM((width, 2 * LANES), BF16),
        "attn": pltpu.VMEM((HD, width), BF16),
        "mix": pltpu.VMEM((channels, width), BF16),
        "xn": pltpu.VMEM((256, width), BF16),
        "xm": pltpu.VMEM((128, width), BF16),
        "kall": pltpu.VMEM((CORES * passages, prows, HD), BF16),
        "vall": pltpu.VMEM((CORES * passages, LANES, 2 * prows), BF16),
        "outs": pltpu.VMEM((slots + 1, LANES, LANES), BF16),
        "ml": pltpu.VMEM((slots + 1, 2, LANES), F32),
        "tabv": pltpu.VMEM(table.shape, jnp.int32),
        "tabs": pltpu.SMEM(table.shape, jnp.int32),
        "acc": pltpu.VMEM((ring, blocks, LANES, LANES), BF16),
        "stats": pltpu.VMEM((ring, blocks, 2, LANES), F32),
        "ydata": pltpu.VMEM((2, blocks, half, LANES, LANES), BF16),
        "ystat": pltpu.VMEM((2, blocks, half, 2, LANES), F32),
        "jdata": pltpu.VMEM((blocks, LANES, LANES), BF16),
        "jstat": pltpu.VMEM((blocks, 2, LANES), F32),
        "rows_a": pltpu.VMEM((xhalf + 1, 2 * block_len, HD), BF16),
        "padded": pltpu.VMEM((groups, 128 + 32, LANES), F32),
        "conv": pltpu.VMEM((groups, 128, LANES), F32),
        "sums": pltpu.VMEM((2 * groups, 128), F32),
        "allsums": pltpu.VMEM((n_tp, 2 * groups, 128), F32),
        "act": pltpu.VMEM((blocks, block_len, channels), BF16),
        "xdata": pltpu.VMEM((2, xhalf, tiles, mine, 512), BF16),
        "xfirst": pltpu.VMEM((tiles, mine, 512), BF16),
        "load_sem": dma((7 + groups + passages + len(small) + 1,)),
        "q_send": dma((2, half, groups)),
        "q_recv": dma((2, half, groups)),
        "kv_send": dma((2, passages)),
        "kv_recv": dma((2, passages)),
        "t_send": dma((ring - 1,)),
        "t_recv": dma((ring - 1,)),
        "s_sem": dma((2,)),
        "y_send": dma((2, blocks, half, 2)),
        "y_recv": dma((2, blocks, half, 2)),
        "j_send": dma((blocks, 2)),
        "j_recv": dma((blocks, 2)),
        "x_send": dma((2, xhalf, tiles)),
        "x_recv": dma((2, xhalf, tiles)),
        "c_send": dma((n_tp - 1,)),
        "c_recv": dma((n_tp - 1,)),
        "qall": None,
    }
    scratch = {**{n[:-4]: pltpu.VMEM(a.shape, a.dtype) for n, a in small.items()},
               "table": pltpu.VMEM(table.shape, table.dtype), **scratch}
    names = list(big) + list(small) + ["table_hbm", "out"] + list(scratch)
    shapes = [s for n, s in scratch.items() if n != "qall"]
    shapes += [pltpu.VMEM((blocks, block_len, HD), BF16) for _ in range(ring)]
    vmem = pl.BlockSpec(memory_space=pltpu.VMEM)
    return pl.pallas_call(
        functools.partial(whole_kernel, names, n_st, n_tp, slots, blocks, per_block),
        out_shape=jax.ShapeDtypeStruct((mine, width), BF16),
        in_specs=[pl.BlockSpec(memory_space=pl.ANY)] * (len(big) + len(small) + 1),
        out_specs=vmem,
        scratch_shapes=shapes,
        compiler_params=pltpu.CompilerParams(
            collective_id=0, has_side_effects=True, vmem_limit_bytes=66_000_000
        ),
        name="whole",
    )(*big.values(), *small.values(), table)


def request_tables(passage_ids, chips, chip_passages, slots):
    blocks, per_block = passage_ids.shape
    flat = passage_ids.reshape(-1)
    number = jnp.arange(flat.shape[0])
    chip_of = flat // chip_passages
    local_of = flat - chip_of * chip_passages
    earlier = (chip_of[:, None] == chip_of[None, :]) & (number[None, :] < number[:, None])
    rank = jnp.sum(earlier.astype(jnp.int32), axis=1)
    here = jnp.arange(chips)[:, None] == chip_of[None, :]
    taken = here[:, None, :] & (jnp.arange(slots)[None, :, None] == rank[None, None, :])
    block_of = jnp.sum(jnp.where(taken, number // per_block, 0), axis=2)
    passage_of = jnp.sum(jnp.where(taken, local_of, 0), axis=2)
    slot_of = jnp.where(here, rank, slots)
    table = jnp.concatenate([block_of, passage_of, slot_of], axis=1).astype(jnp.int32)
    return jnp.pad(table, ((0, 0), (0, LANES - table.shape[1])))[:, None, :]


def local(
    tokens, store, passage_ids, mix_gain, glu_value, glu_gate, conv_taps, channel_gain, mix_out,
    query_gain, passage_gain, query_proj, key_proj, value_proj, attn_out, blend_gain,
):
    owners = lax.axis_size("st")
    blocks, per_block = passage_ids.shape
    slots = CORES * (2 * blocks * per_block // owners)
    table = request_tables(passage_ids, owners // CORES, CORES * store.shape[0], slots)
    big = {
        "tok_hbm": tokens, "store_hbm": store, "wq_hbm": query_proj, "wk_hbm": key_proj, "wv_hbm": value_proj,
        "gv_hbm": glu_value, "gg_hbm": glu_gate, "attn_hbm": attn_out, "mix_hbm": mix_out,
    }
    small = {
        "qgain_hbm": query_gain[None], "pgain_hbm": passage_gain[None], "mgain_hbm": mix_gain[None], "taps_hbm": conv_taps,
        "cgain_hbm": channel_gain[None], "blend_hbm": blend_gain[None],
    }
    return whole(table, slots, blocks, per_block, big, small)


def solution(mesh):
    in_specs = (
        P(("grp", "st"), None),
        P(("grp", "st"), None, None),
        P(("grp", "st"), None),
        P(),
        P(None, "tp"),
        P(None, "tp"),
        P(None, "tp"),
        P("tp"),
        P("tp", None),
        P(),
        P(),
        P(None, "tp"),
        P(None, "tp"),
        P(None, "tp"),
        P("tp", None),
        P(),
    )
    out_specs = P(("grp", "st", "tp"), None)
    return jax.shard_map(local, mesh=mesh, in_specs=in_specs, out_specs=out_specs, check_vma=False)
```

time: 228 us -> 92.1 us (0.40); the launches traced: 224 us -> 91.3 us
  Pallas kernels: 0 us -> 87.5 us
  blocking collectives: 68.8 us -> 0 us
  waiting for transfers between devices: 57.9 us -> 0 us
  starting transfers between devices: 41.6 us -> 0 us
  matrix products: 21.6 us -> 0 us
  local copies, waits for them, and re-layouts: 20.8 us -> 3.11 us
  other arithmetic: 12.8 us -> 0.64 us
    pallas_call x0 -> x1, Pallas kernels: none -> 87.5 us  [whole(): pl.pallas_call(functools.partial(whole_kernel, names, n_st, n_tp, slots,...]
    all_to_all x4 -> x0, waiting for transfers between devices: 57.9 us -> none  [the longest x1 32.7 us: local(): lax.all_to_all(slot_queries.reshape(owners, capacity, block_len, head_wid...]
    all_to_all x1 -> x0, blocking collectives: 54.5 us -> none  [sent_and_summed(): pieces = lax.all_to_all(cut_along(x, dim, size), axis, 0, 0, tiled=True)]
    all_to_all x4 -> x0, starting transfers between devices: 41.6 us -> none  [the longest x1 21.5 us: local(): lax.all_to_all(slot_ids, 'st', split_axis=0, concat_axis=0, tiled=True)]
    dot_general x10 -> x0, matrix products: 21.6 us -> none  [the longest x1 4.77 us: passage_attention(): jnp.einsum('ghqr,grhd->gqhd', weights, value_heads, preferred_element_typ...]
    psum x1 -> x0, blocking collectives: 14.2 us -> none  [local(): lax.psum((jnp.sum(conv_rows, axis=1), jnp.sum(conv_rows * conv_rows, axis...]
    reduce_sum x7 -> x2, other arithmetic: 9.03 us -> 0.53 us  [the longest x1 0.35 us: request_tables(): block_of = jnp.sum(jnp.where(taken, number // per_block, 0), axis=2)]
    gather x4 -> x0, local copies, waits for them, and re-layouts: 8.12 us -> none  [the longest x1 5.37 us: local(): served = memory[asked.reshape(owners * capacity)]]
  transfers between devices with their start and end apart: 4 -> 0, of which waited for: 3 -> 0; matrix products, arithmetic and copies ran while one was open for 17% -> 0% of each run, Pallas kernels for 0% -> 0%
where the time goes in v2:
time: 92.1 us; the launch traced here: 91.3 us
  Pallas kernels  87.5 us (95%)
  local copies, waits for them, and re-layouts  3.11 us (3%)
    pallas_call x1, Pallas kernels, whole(): pl.pallas_call(functools.partial(whole_kernel, names, n_st, n_tp, slots,...  87.5 us
    unnamed x2, local copies, waits for them, and re-layouts  2.43 us

profile of v2, /device:TPU:528, one launch (start us, length us, event | category | flops | bytes accessed | tf_op | source)
XLA Modules:
  0.0 91.3 jit_solution(11118360321838399440)
XLA Ops:
  0.0 0.8 copy.19
  0.8 0.1 reshape.101
  0.9 0.2 convert_reduce_fusion
  1.1 0.4 fusion
  1.4 0.1 pad_add_fusion
  1.5 0.6 pad.4
  2.1 87.5 %whole.1 = bf16[64,2048]{1,0:T(8,128)(2,1)} custom-call(bf16[512,2048]{1,0:T(8,128)(2,1)} %refs_0_.1, bf16[8,128,2048]{2,1,0:T(8,128)(2,1)} %refs_1_.1, bf16[2048,256]{1,0:T(8,128)(2,1)} %refs_2_.1, bf16[2048,256]{1,0:T(8,128)(2,1)} %refs_3_.1, bf16[2048,256]{1,0:T(8,128)(2,1)} %refs_4_.1, bf16[2048,128]{1,0:T(8,128)(2,1)} %refs_5_.1, ...), custom_call_target="tpu_custom_call" | custom-call | tf_op jit(solution)/shard_map/whole/pallas_call | solution.py:584
  89.6 1.7 %copy.21 = bf16[64,2048]{1,0:T(8,128)(2,1)} copy(bf16[64,2048]{1,0:T(8,128)(2,1)} %whole.1) | data formatting | bytes 524288
  (4 shorter events, 0.0 us)

commit v3 on v2

--- a/solution.py
+++ b/solution.py
@@ -14,7 +14,7 @@
 LANES = 128
 EPS = 1e-06
 EMPTY = -1e30
-BACKLOG = {5: 9.0, 6: 9.0, 7: 1.2, 8: 0.0, 9: 0.0}
+BACKLOG = {6: 9.0, 7: 0.8, 8: 0.15, 9: 0.15}
 MESH = pl.DeviceIdType.MESH
 F32 = jnp.float32
 BF16 = jnp.bfloat16
@@ -72,15 +72,16 @@
                 if all(a in done for a in after) and all(g in arrival for g in gets):
                     ready = max([clock] + [arrival[g] for g in gets])
                     if rank in backlog:
-                        ready = max([ready] + [free.get(link, 0.0) - backlog[rank] for _, link, _, _ in sends])
+                        ready = max([ready] + [free.get(link, 0.0) - backlog[rank] for _, link, *_ in sends])
                     if best is None or (ready, rank) < best[0]:
                         best = ((ready, rank), name)
             (ready, _), name = best
             _, time, _, _, _, sends = self.steps[name]
             clock = ready + time
-            for message, link, wire, late in sends:
+            for message, link, wire, late, *hops in sends:
                 free[link] = max(free.get(link, 0.0), clock) + wire
                 arrival[message] = free[link] + late
+                free[link] += wire * (hops[0] - 1 if hops else 0)
             done.add(name)
             left.remove(name)
             order.append((name, ready, clock))
@@ -90,7 +91,7 @@
 def step_plan(k):
     plan = Plan()
     ring, half, groups, xhalf = k.ring, k.half, k.groups, k.xhalf
-    hop_late, far_late, q_wire, y_wire, x_wire = 2.3, 0.75, 1.4, 0.72, 1.4
+    hop_late, far_late, q_wire, y_wire, x_wire = 2.4, 0.75, 1.4, 0.72, 1.4
     for g in range(groups):
         plan.add(
             ("q", g), functools.partial(k.queries, g), 0.76, 1, [("q", g - 1)] if g else [],
@@ -109,9 +110,10 @@
                 )
     pairs = list(range(0, k.passages, 2))
     for p in pairs:
-        plan.add(("norm", p), functools.partial(k.norm_passages, p), 0.75, 20, [("v", p - 2)] if p else [("q", groups - 1)])
-        plan.add(("k", p), functools.partial(k.keys, p), 0.5, 20, [("norm", p)])
-        plan.add(("v", p), functools.partial(k.values, p), 0.65, 20, [("k", p)], sends=[(("kv", p), ("core",), 0.4, 1.0)])
+        if p == 0:
+            plan.add(("norm", p), functools.partial(k.norm_passages, p), 1.0, 20, [("q", groups - 1)])
+        plan.add(("k", p), functools.partial(k.keys, p), 0.77, 20, [("v", p - 2) if p else ("norm", p)])
+        plan.add(("v", p), functools.partial(k.values, p), 0.86, 20, [("k", p)], sends=[(("kv", p), ("core",), 0.4, 1.0)])
     plan.add(("here",), k.all_here, 0.65, 21, [("v", p) for p in pairs], gets=[("kv", p) for p in pairs])
     for rel in range(ring):
         hop = min(rel, ring - rel)
@@ -122,26 +124,31 @@
         else:
             hands = []
         plan.add(("slots", rel), functools.partial(k.attend, rel), 0.6, 19 - hop, [("here",)] + hands)
-        plan.add(("attend", rel), functools.partial(k.join, rel), 0.4, 1, [("slots", rel)])
-    for c, chunk in enumerate(k.chunks):
+        plan.add(("attend", rel), functools.partial(k.join, rel), 0.3, 1, [("slots", rel)])
+    for rel in range(1, ring):
+        hop = min(rel, ring - rel)
+        plan.add(
+            ("direct", rel), functools.partial(k.direct, rel), 0.04, 2, [("attend", rel)],
+            sends=[(("direct", ring - rel), ("y", 0 if rel <= half else 1), y_wire, hop_late + far_late * (hop - 1), hop)],
+        )
+    for c, chunk in enumerate(k.chunks[1:], 1):
         for p in chunk:
             joined = k.join_side(p)
             if joined is not None:
                 plan.add(
-                    ("join", p), functools.partial(k.join_late, p), 0.03, 5 + c, [("attend", half)],
-                    sends=[(("join", p), ("y", joined), y_wire * (half - k.join_hop(p)),
-                            hop_late + far_late * (half - k.join_hop(p) - 1))],
+                    ("join", p), functools.partial(k.join_late, p), 0.04, 5 + c, [("attend", half)],
+                    sends=[(("join", p), ("y", joined), y_wire, hop_late + far_late * (half - 2), half - 1)],
                 )
             for side in range(2):
                 far = k.start_of(side, p)
                 for d in range(far, 0, -1):
                     rel = d if side == 0 else ring - d
                     gets = [] if d == far else [("y", side, p, d)]
-                    if joined == side and d == k.join_hop(p):
+                    if joined == side and d == 1:
                         gets = gets + [("join", p)]
                     plan.add(
                         ("y", side, p, d),
-                        functools.partial(k.y_start if d == far else k.y_stage, side, p, d), 0.03 if d == far else 0.1,
+                        functools.partial(k.y_start if d == far else k.y_stage, side, p, d), 0.04 if d == far else 0.06,
                         5 + c, [("attend", rel)], gets=gets,
                         sends=[(("y", side, p, d - 1), ("y", side), y_wire, hop_late)],
                     )
@@ -152,8 +159,10 @@
              sends=[(("sums",), ("x", 2), 0.5, 5.0)])
     plan.add(("act",), k.activations, 0.4, 4, gets=[("sums",)])
     for c, chunk in enumerate(k.chunks):
-        gets = [("y", side, p, 0) for p in chunk for side in range(2)]
-        gets += [("join", p) for p in chunk if k.join_side(p) is not None and k.join_hop(p) == 0]
+        if c == 0:
+            gets = [("direct", rel) for rel in range(1, ring)]
+        else:
+            gets = [("y", side, p, 0) for p in chunk for side in range(2)]
         plan.add(("home", c), functools.partial(k.home, c), 0.3, 4, [("attend", 0)], gets=gets)
         dist = xhalf - c
         for t in range(k.tiles):
@@ -189,7 +198,7 @@
         self.core, self.y_me = lax.rem(self.me, CORES), self.me // CORES
         self.partner = self.me + 1 - 2 * self.core
         self.right, self.left = self.chip(1), self.chip(self.ring - 1)
-        self.sends, self.loads = [], []
+        self.waiting, self.unused, self.loads, self.clock = [], list(range(refs["send_sem"].shape[0])), [], 0.0
         self.early = 2
         self.places = order_of(n_tp)
         self.chunks = [[0]] + [[2 * j - 1, 2 * j] for j in range(1, self.xhalf)] + [[n_tp - 1]]
@@ -204,9 +213,26 @@
     def column(self, d):
         return lax.rem(self.x_me + d, self.n_tp)
 
-    def send(self, copy):
-        copy.start()
-        self.sends.append(copy)
+    def send(self, src, dst, recv_sem, **target):
+        self.send_all([(src, dst)], recv_sem, **target)
+
+    def send_all(self, pairs, recv_sem, **target):
+        if not self.unused:
+            self.settle()
+        at = self.unused.pop(0)
+        sem = self.send_sem.at[at]
+        for src, dst in pairs:
+            remote(src, dst, sem, recv_sem, **target).start()
+        whole = self.both if len(pairs) > 1 else pairs[0][0]
+        self.waiting.append((self.clock, remote(whole, whole, sem, recv_sem, **target), at))
+
+    def settle(self):
+        _, copy, at = self.waiting.pop(0)
+        copy.wait_send()
+        self.unused.append(at)
+
+    def got(self, ref, recv_sem):
+        remote(ref, ref, self.send_sem.at[0], recv_sem, st=self.partner).wait_recv()
 
     def load(self, src, dst):
         copy = pltpu.make_async_copy(src, dst, self.load_sem.at[len(self.loads)])
@@ -224,7 +250,7 @@
         self.first_loads = [small("qgain"), self.load(self.wq_hbm, self.wq)]
         rows = lambda g: pl.ds(g * 128, 128)
         self.tok_loads = [self.load(self.tok_hbm.at[rows(g)], self.tok.at[rows(g)]) for g in range(self.groups)]
-        self.table_load = small("table")
+        self.ids_load = small("ids")
         self.kv_loads = [small("pgain"), self.load(self.wk_hbm, self.wk), self.load(self.wv_hbm, self.wv)]
         self.store_loads = [
             self.load(self.store_hbm.at[p], self.store.at[pl.ds(p * 128, 128)]) for p in range(self.passages)
@@ -247,12 +273,30 @@
         self.ml[s, 1:2] = jnp.zeros((1, LANES), F32)
         self.padded[...] = jnp.zeros(self.padded.shape, F32)
 
+    def make_table(self):
+        self.ids_load.wait()
+        chip = lax.broadcasted_iota(jnp.int32, (self.ring, LANES), 0)
+        lane = lax.broadcasted_iota(jnp.int32, (self.ring, LANES), 1)
+        used = jnp.zeros((self.ring, LANES), jnp.int32)
+        table = jnp.zeros((self.ring, LANES), jnp.int32)
+        held = CORES * self.passages
+        for n in range(self.blocks * self.per_block):
+            wanted = self.ids[n % self.per_block, n // self.per_block]
+            owner = wanted // held
+            here = (chip == owner) & (used < self.slots)
+            table = jnp.where(here & (lane == used), n // self.per_block, table)
+            table = jnp.where(here & (lane == self.slots + used), wanted - owner * held, table)
+            table = jnp.where(lane == 2 * self.slots + n, jnp.where(here, used, self.slots), table)
+            used = used + jnp.where(here, 1, 0)
+        for i in range(self.ring):
+            self.table[i] = table[i : i + 1]
+
     def entered(self):
-        self.table_load.wait()
+        self.make_table()
         pl.semaphore_wait(pltpu.get_barrier_semaphore(), self.ring + self.n_tp - 1)
         for d in range(1, self.ring):
-            self.send(remote(self.table.at[lax.rem(self.y_me + d, self.ring)], self.tabv.at[self.ring - d],
-                             self.t_send.at[d - 1], self.t_recv.at[self.ring - d - 1], st=self.chip(d)))
+            self.send(self.table.at[lax.rem(self.y_me + d, self.ring)], self.tabv.at[self.ring - d], self.t_recv.at[0],
+                      st=self.chip(d))
         self.own_table = pltpu.make_async_copy(self.table.at[self.y_me], self.tabv.at[0], self.s_sem.at[1])
         self.own_table.start()
 
@@ -264,10 +308,10 @@
         self.tok_loads[g].wait()
         if g == 0:
             self.first_loads[0].wait()
-        normed_rows(self.xn.at[pl.ds(0, 128)], self.tok.at[pl.ds(g * 128, 128)], self.qgain, 128, unroll=4)
+        normed_rows(self.xq, self.tok.at[pl.ds(g * 128, 128)], self.qgain, 128, unroll=4)
         if g == 0:
             self.first_loads[1].wait()
-        q = jnp.dot(self.xn[pl.ds(0, 128), :], self.wq[...], preferred_element_type=F32).astype(BF16)
+        q = jnp.dot(self.xq[...], self.wq[...], preferred_element_type=F32).astype(BF16)
         n = self.block_len
         for i in range(self.per_group):
             self.qall[0][self.per_group * g + i] = q[i * n : (i + 1) * n]
@@ -275,55 +319,62 @@
             with jax.named_scope("entry"):
                 self.entered()
         for side, rel, who in ((0, self.ring - 1, self.right), (1, 1, self.left)):
-            self.send(remote(self.part(0, g), self.part(rel, g), self.q_send.at[side, 0, g], self.q_recv.at[side, 0, g],
-                             st=who))
+            self.send(self.part(0, g), self.part(rel, g), self.q_recv.at[self.q_sem(side, 1, g)], st=who)
 
     def hand_on(self, side, hop, g, on):
         rel = self.ring - hop if side == 0 else hop
         here = self.part(rel, g)
-        remote(here, here, self.q_send.at[side, hop - 1, g], self.q_recv.at[side, hop - 1, g], st=self.right).wait_recv()
+        self.got(here, self.q_recv.at[self.q_sem(side, hop, g)])
         if on:
             there = self.part(rel - 1 if side == 0 else rel + 1, g)
-            self.send(remote(here, there, self.q_send.at[side, hop, g], self.q_recv.at[side, hop, g],
-                             st=self.right if side == 0 else self.left))
+            self.send(here, there, self.q_recv.at[self.q_sem(side, hop + 1, g)],
+                      st=self.right if side == 0 else self.left)
+
+    def q_sem(self, side, hop, g):
+        last = (self.half - 1) * self.groups
+        each = last + self.groups // 2
+        return side * each + ((hop - 1) * self.groups + g if hop < self.half else last + g % (self.groups // 2))
 
 
     def norm_passages(self, p):
-        for i in range(2):
-            self.store_loads[p + i].wait()
-        if p == 0:
-            for copy in self.kv_loads:
-                copy.wait()
-        normed_rows(self.xn, self.store.at[pl.ds(p * 128, 256)], self.pgain, 256)
-
-    def share(self, j, ref, at, p):
-        self.send(remote(ref.at[at], ref.at[at], self.kv_send.at[j, p], self.kv_recv.at[j, p], st=self.partner))
+        for copy in self.kv_loads + self.store_loads[:2]:
+            copy.wait()
+        self.norm_half(p, 0, unroll=2)
+        self.norm_half(p, 1, unroll=2)
+
+    def norm_half(self, p, i, unroll=8):
+        if p < self.passages:
+            if p:
+                self.store_loads[p + i].wait()
+            normed_rows(self.xn.at[p // 2 % 2, pl.ds(i * 128, 128)], self.store.at[pl.ds((p + i) * 128, 128)], self.pgain,
+                        128, unroll=unroll)
+
+    def share(self, j, ref, p):
+        both = ref.at[pl.ds(self.core * self.passages + p, 2)]
+        self.send(both, both, self.kv_recv.at[j], st=self.partner)
 
     def keys(self, p):
-        k = jnp.dot(self.xn[...], self.wk[...], preferred_element_type=F32).astype(BF16)
+        self.norm_half(p + 2, 0)
+        k = jnp.dot(self.xn[p // 2 % 2], self.wk[...], preferred_element_type=F32).astype(BF16)
         for i in range(2):
             at = self.core * self.passages + p + i
             self.kall[at] = k[i * 128 : (i + 1) * 128]
-            self.share(0, self.kall, at, p + i)
+        self.share(0, self.kall, p)
 
     def values(self, p):
-        v = jnp.dot(self.xn[...], self.wv[...], preferred_element_type=F32)
+        self.norm_half(p + 2, 1)
+        v = jnp.dot(self.xn[p // 2 % 2], self.wv[...], preferred_element_type=F32)
         for i in range(2):
             at = self.core * self.passages + p + i
             w = v[i * 128 : (i + 1) * 128]
             self.vall[at] = jnp.concatenate([w[:, :LANES].T, w[:, LANES:].T], axis=1).astype(BF16)
-            self.share(1, self.vall, at, p + i)
+        self.share(1, self.vall, p)
 
     def all_here(self):
-        for p in range(self.passages):
-            other = (1 - self.core) * self.passages + p
-            for j, ref in enumerate((self.kall, self.vall)):
-                remote(ref.at[other], ref.at[other], self.kv_send.at[j, p], self.kv_recv.at[j, p],
-                       st=self.partner).wait_recv()
+        for j, ref in enumerate((self.kall, self.vall)):
+            self.got(ref.at[pl.ds((1 - self.core) * self.passages, self.passages)], self.kv_recv.at[j])
         self.own_table.wait()
-        for d in range(1, self.ring):
-            here = self.tabv.at[d]
-            remote(here, here, self.t_send.at[d - 1], self.t_recv.at[d - 1], st=self.partner).wait_recv()
+        self.got(self.tabv.at[pl.ds(1, self.ring - 1)], self.t_recv.at[0])
         to_scalar = pltpu.make_async_copy(self.tabv, self.tabs, self.s_sem.at[0])
         to_scalar.start()
         to_scalar.wait()
@@ -348,7 +399,7 @@
     def join(self, rel):
         slots, tabs, ml, outs = self.slots, self.tabs, self.ml, self.outs
 
-        @pl.loop(0, self.blocks)
+        @pl.loop(0, self.blocks, unroll=4)
         def _(distance):
             b = lax.rem(self.x_me + distance, self.blocks)
             at = [tabs[rel, 0, 2 * slots + b * self.per_block + j] for j in range(self.per_block)]
@@ -365,18 +416,18 @@
 
     def y_out(self, side, p, d, num, stat):
         who = self.right if side == 0 else self.left
-        for i, (src, dst) in enumerate(((num, self.ydata), (stat, self.ystat))):
-            self.send(remote(src, dst.at[side, p, d - 1], self.y_send.at[side, p, d - 1, i],
-                             self.y_recv.at[side, p, d - 1, i], st=who))
+        pairs = [(num, self.ydata.at[side, p, d - 1]), (stat, self.ystat.at[side, p, d - 1])]
+        self.send_all(pairs, self.y_recv.at[self.y_sem(side, p, d - 1)], st=who)
+
+    def y_sem(self, side, p, d):
+        return sum(self.start_of(i, q) for q in range(1, p) for i in range(2)) + side * self.start_of(0, p) + d
 
     def y_start(self, side, p, d):
         rel = d if side == 0 else self.ring - d
         self.y_out(side, p, d, self.acc.at[rel, p], self.stats.at[rel, p])
 
     def y_arrived(self, side, p, d):
-        for i, ref in enumerate((self.ydata, self.ystat)):
-            here = ref.at[side, p, d]
-            remote(here, here, self.y_send.at[side, p, d, i], self.y_recv.at[side, p, d, i], st=self.right).wait_recv()
+        self.got(self.both, self.y_recv.at[self.y_sem(side, p, d)])
         stat = self.ystat.at[side, p, d]
         return self.ydata[side, p, d].astype(F32), stat[0:1], stat[1:2]
 
@@ -385,7 +436,7 @@
 
     def y_stage(self, side, p, d):
         so_far = merged(self.y_arrived(side, p, d), self.own(d if side == 0 else self.ring - d, p))
-        if self.join_side(p) == side and self.join_hop(p) == d:
+        if d == 1 and self.join_side(p) == side:
             so_far = merged(so_far, self.joined(p))
         num, best, total = so_far
         self.ydata[side, p, d] = num.astype(BF16)
@@ -394,31 +445,37 @@
         self.y_out(side, p, d, self.ydata.at[side, p, d], self.ystat.at[side, p, d])
 
     def join_side(self, p):
-        early = [q for chunk in self.chunks[: self.early] for q in chunk]
-        return (early.index(p) + 1) % 2 if p in early else None
-
-    def join_hop(self, p):
-        return 0 if p == self.chunks[0][0] else 1
+        early = [q for chunk in self.chunks[1 : self.early] for q in chunk]
+        return early.index(p) % 2 if p in early else None
 
     def join_late(self, p):
         side = self.join_side(p)
-        hops = self.half - self.join_hop(p)
+        hops = self.half - 1
         who = self.chip(hops if side == 0 else self.ring - hops)
-        for i, (src, dst) in enumerate(((self.acc, self.jdata), (self.stats, self.jstat))):
-            self.send(remote(src.at[self.half, p], dst.at[p], self.j_send.at[p, i], self.j_recv.at[p, i], st=who))
+        pairs = [(self.acc.at[self.half, p], self.jdata.at[p]), (self.stats.at[self.half, p], self.jstat.at[p])]
+        self.send_all(pairs, self.j_recv.at[p], st=who)
 
     def joined(self, p):
-        for i, ref in enumerate((self.jdata, self.jstat)):
-            here = ref.at[p]
-            remote(here, here, self.j_send.at[p, i], self.j_recv.at[p, i], st=self.right).wait_recv()
+        self.got(self.both, self.j_recv.at[p])
         stat = self.jstat.at[p]
         return self.jdata[p].astype(F32), stat[0:1], stat[1:2]
 
+    def direct(self, rel):
+        p = self.chunks[0][0]
+        at = self.ring - rel
+        pairs = [(self.acc.at[rel, p], self.ddata.at[at]), (self.stats.at[rel, p], self.dstat.at[at])]
+        self.send_all(pairs, self.d_recv.at[at - 1], st=self.chip(rel))
+
     def home(self, c):
         for i, p in enumerate(self.chunks[c]):
-            so_far = merged(merged(self.y_arrived(0, p, 0), self.own(0, p)), self.y_arrived(1, p, 0))
-            if self.join_side(p) is not None and self.join_hop(p) == 0:
-                so_far = merged(so_far, self.joined(p))
+            if c == 0:
+                so_far = self.own(0, p)
+                for rel in range(1, self.ring):
+                    self.got(self.both, self.d_recv.at[rel - 1])
+                    stat = self.dstat.at[rel]
+                    so_far = merged(so_far, (self.ddata[rel].astype(F32), stat[0:1], stat[1:2]))
+            else:
+                so_far = merged(merged(self.y_arrived(0, p, 0), self.own(0, p)), self.y_arrived(1, p, 0))
             num, best, total = so_far
             t = (num / total).T.astype(BF16)
             n = self.block_len
@@ -450,14 +507,12 @@
 
     def send_sums(self):
         for d in range(1, self.n_tp):
-            self.send(remote(self.sums, self.allsums.at[self.n_tp - d], self.c_send.at[d - 1],
-                             self.c_recv.at[self.n_tp - d - 1], tp=self.column(d)))
+            self.send(self.sums, self.allsums.at[self.n_tp - d], self.c_recv.at[0], tp=self.column(d))
 
     def activations(self):
         total = self.sums[...]
+        self.got(self.allsums.at[pl.ds(1, self.n_tp - 1)], self.c_recv.at[0])
         for d in range(1, self.n_tp):
-            here = self.allsums.at[d]
-            remote(here, here, self.c_send.at[d - 1], self.c_recv.at[d - 1], tp=self.column(1)).wait_recv()
             total = total + self.allsums[d]
         groups = self.groups
         mean = total[:groups] / CA
@@ -482,8 +537,7 @@
             self.rows_a[c, pl.ds(0, n * len(chunk)), :], self.attn[:, at], preferred_element_type=F32
         )
         for side in gets:
-            here = self.xdata.at[side, k, t]
-            remote(here, here, self.x_send.at[side, k, t], self.x_recv.at[side, k, t], tp=self.column(1)).wait_recv()
+            self.got(self.xdata.at[side, k, t], self.x_recv.at[self.x_sem(side, k, t)])
         if k == 0:
             y = y + self.xdata[0, k, t].astype(F32) + self.xdata[1, k, t].astype(F32)
             self.out[:, at] = y.astype(BF16)
@@ -494,9 +548,13 @@
                 mine = mine + self.xdata[side, k, t].astype(F32)
             slot = self.xdata.at[side, k, t] if k < self.xhalf else self.xfirst.at[t]
             slot[...] = mine.astype(BF16)
-            self.send(remote(slot, self.xdata.at[side, k - 1, t], self.x_send.at[side, k - 1, t],
-                             self.x_recv.at[side, k - 1, t],
-                             tp=self.column(1 if side == 0 else self.n_tp - 1)))
+            self.send(slot, self.xdata.at[side, k - 1, t], self.x_recv.at[self.x_sem(side, k - 1, t)],
+                      tp=self.column(1 if side == 0 else self.n_tp - 1))
+
+    def x_sem(self, side, k, t):
+        return side * (self.xhalf - 1) * self.tiles + k * self.tiles + t if k < self.xhalf - 1 else (
+            2 * (self.xhalf - 1) * self.tiles + t
+        )
 
 
 def whole_kernel(names, n_st, n_tp, slots, blocks, per_block, *refs):
@@ -508,14 +566,20 @@
     plan = step_plan(k)
     with jax.named_scope("enter"):
         k.enter()
-    for name, _, _ in plan.order(BACKLOG):
+    for name, ready, end in plan.order(BACKLOG):
+        gap = ready - k.clock
+        while gap > 0.1 and k.waiting and k.waiting[0][0] < k.clock - 8.0:
+            k.settle()
+            gap -= 0.03
         with jax.named_scope("_".join(str(part) for part in name)):
             plan.steps[name][0]()
-    for copy in k.sends:
-        copy.wait_send()
-
-
-def whole(table, slots, blocks, per_block, big, small):
+        k.clock = end
+    with jax.named_scope(f"tail_{len(k.waiting)}"):
+        while k.waiting:
+            k.settle()
+
+
+def whole(ids, slots, blocks, per_block, big, small):
     n_st, n_tp = lax.axis_size("st"), lax.axis_size("tp")
     ring, half, xhalf = n_st // CORES, n_st // CORES // 2, n_tp // 2
     rows, width = big["tok_hbm"].shape
@@ -535,18 +599,22 @@
         "wglu": pltpu.VMEM((width, 2 * LANES), BF16),
         "attn": pltpu.VMEM((HD, width), BF16),
         "mix": pltpu.VMEM((channels, width), BF16),
-        "xn": pltpu.VMEM((256, width), BF16),
+        "xq": pltpu.VMEM((128, width), BF16),
+        "xn": pltpu.VMEM((2, 256, width), BF16),
         "xm": pltpu.VMEM((128, width), BF16),
         "kall": pltpu.VMEM((CORES * passages, prows, HD), BF16),
         "vall": pltpu.VMEM((CORES * passages, LANES, 2 * prows), BF16),
         "outs": pltpu.VMEM((slots + 1, LANES, LANES), BF16),
         "ml": pltpu.VMEM((slots + 1, 2, LANES), F32),
-        "tabv": pltpu.VMEM(table.shape, jnp.int32),
-        "tabs": pltpu.SMEM(table.shape, jnp.int32),
+        "tabv": pltpu.VMEM((ring, 1, LANES), jnp.int32),
+        "tabs": pltpu.SMEM((ring, 1, LANES), jnp.int32),
         "acc": pltpu.VMEM((ring, blocks, LANES, LANES), BF16),
         "stats": pltpu.VMEM((ring, blocks, 2, LANES), F32),
         "ydata": pltpu.VMEM((2, blocks, half, LANES, LANES), BF16),
         "ystat": pltpu.VMEM((2, blocks, half, 2, LANES), F32),
+        "ddata": pltpu.VMEM((ring, LANES, LANES), BF16),
+        "dstat": pltpu.VMEM((ring, 2, LANES), F32),
+        "both": pltpu.VMEM((1 + LANES * LANES * 2 // (2 * LANES * 4), 2, LANES), F32),
         "jdata": pltpu.VMEM((blocks, LANES, LANES), BF16),
         "jstat": pltpu.VMEM((blocks, 2, LANES), F32),
         "rows_a": pltpu.VMEM((xhalf + 1, 2 * block_len, HD), BF16),
@@ -558,57 +626,35 @@
         "xdata": pltpu.VMEM((2, xhalf, tiles, mine, 512), BF16),
         "xfirst": pltpu.VMEM((tiles, mine, 512), BF16),
         "load_sem": dma((7 + groups + passages + len(small) + 1,)),
-        "q_send": dma((2, half, groups)),
-        "q_recv": dma((2, half, groups)),
-        "kv_send": dma((2, passages)),
-        "kv_recv": dma((2, passages)),
-        "t_send": dma((ring - 1,)),
-        "t_recv": dma((ring - 1,)),
+        "send_sem": dma((48,)),
+        "q_recv": dma((2 * ((half - 1) * groups + groups // 2),)),
+        "kv_recv": dma((2,)),
+        "t_recv": dma((1,)),
         "s_sem": dma((2,)),
-        "y_send": dma((2, blocks, half, 2)),
-        "y_recv": dma((2, blocks, half, 2)),
-        "j_send": dma((blocks, 2)),
-        "j_recv": dma((blocks, 2)),
-        "x_send": dma((2, xhalf, tiles)),
-        "x_recv": dma((2, xhalf, tiles)),
-        "c_send": dma((n_tp - 1,)),
-        "c_recv": dma((n_tp - 1,)),
+        "y_recv": dma(((blocks - 1) * (2 * half - 1),)),
+        "d_recv": dma((ring - 1,)),
+        "j_recv": dma((3,)),
+        "x_recv": dma((2 * (xhalf - 1) * tiles + tiles,)),
+        "c_recv": dma((1,)),
         "qall": None,
     }
     scratch = {**{n[:-4]: pltpu.VMEM(a.shape, a.dtype) for n, a in small.items()},
-               "table": pltpu.VMEM(table.shape, table.dtype), **scratch}
-    names = list(big) + list(small) + ["table_hbm", "out"] + list(scratch)
+               "table": pltpu.VMEM((ring, 1, LANES), jnp.int32), "ids": pltpu.SMEM(ids.shape[::-1], jnp.int32), **scratch}
+    names = list(big) + list(small) + ["ids_hbm", "out"] + list(scratch)
     shapes = [s for n, s in scratch.items() if n != "qall"]
     shapes += [pltpu.VMEM((blocks, block_len, HD), BF16) for _ in range(ring)]
     vmem = pl.BlockSpec(memory_space=pltpu.VMEM)
     return pl.pallas_call(
         functools.partial(whole_kernel, names, n_st, n_tp, slots, blocks, per_block),
         out_shape=jax.ShapeDtypeStruct((mine, width), BF16),
-        in_specs=[pl.BlockSpec(memory_space=pl.ANY)] * (len(big) + len(small) + 1),
+        in_specs=[pl.BlockSpec(memory_space=pltpu.HBM)] * (len(big) + len(small) + 1),
         out_specs=vmem,
         scratch_shapes=shapes,
         compiler_params=pltpu.CompilerParams(
             collective_id=0, has_side_effects=True, vmem_limit_bytes=66_000_000
         ),
         name="whole",
-    )(*big.values(), *small.values(), table)
-
-
-def request_tables(passage_ids, chips, chip_passages, slots):
-    blocks, per_block = passage_ids.shape
-    flat = passage_ids.reshape(-1)
-    number = jnp.arange(flat.shape[0])
-    chip_of = flat // chip_passages
-    local_of = flat - chip_of * chip_passages
-    earlier = (chip_of[:, None] == chip_of[None, :]) & (number[None, :] < number[:, None])
-    rank = jnp.sum(earlier.astype(jnp.int32), axis=1)
-    here = jnp.arange(chips)[:, None] == chip_of[None, :]
-    taken = here[:, None, :] & (jnp.arange(slots)[None, :, None] == rank[None, None, :])
-    block_of = jnp.sum(jnp.where(taken, number // per_block, 0), axis=2)
-    passage_of = jnp.sum(jnp.where(taken, local_of, 0), axis=2)
-    slot_of = jnp.where(here, rank, slots)
-    table = jnp.concatenate([block_of, passage_of, slot_of], axis=1).astype(jnp.int32)
-    return jnp.pad(table, ((0, 0), (0, LANES - table.shape[1])))[:, None, :]
+    )(*big.values(), *small.values(), ids.T)
 
 
 def local(
@@ -618,7 +664,6 @@
     owners = lax.axis_size("st")
     blocks, per_block = passage_ids.shape
     slots = CORES * (2 * blocks * per_block // owners)
-    table = request_tables(passage_ids, owners // CORES, CORES * store.shape[0], slots)
     big = {
         "tok_hbm": tokens, "store_hbm": store, "wq_hbm": query_proj, "wk_hbm": key_proj, "wv_hbm": value_proj,
         "gv_hbm": glu_value, "gg_hbm": glu_gate, "attn_hbm": attn_out, "mix_hbm": mix_out,
@@ -627,7 +672,7 @@
         "qgain_hbm": query_gain[None], "pgain_hbm": passage_gain[None], "mgain_hbm": mix_gain[None], "taps_hbm": conv_taps,
         "cgain_hbm": channel_gain[None], "blend_hbm": blend_gain[None],
     }
-    return whole(table, slots, blocks, per_block, big, small)
+    return whole(passage_ids, slots, blocks, per_block, big, small)
 
 
 def solution(mesh):

time: 92.1 us -> 83.6 us (0.908)
  Pallas kernels: 87.5 us -> 81.8 us
  local copies, waits for them, and re-layouts: 3.11 us -> 1.67 us
    pallas_call x1, Pallas kernels: 87.5 us -> 81.8 us  [whole(): pl.pallas_call(functools.partial(whole_kernel, names, n_st, n_tp, slots,...]
    unnamed x2 -> x1, local copies, waits for them, and re-layouts: 2.43 us -> 1.67 us
where the time goes in v3:
time: 83.6 us; the launch traced here: 83.4 us
  Pallas kernels  81.8 us (98%)
  local copies, waits for them, and re-layouts  1.67 us (2%)
    pallas_call x1, Pallas kernels, whole(): pl.pallas_call(functools.partial(whole_kernel, names, n_st, n_tp, slots,...  81.8 us

profile of v3, /device:TPU:528, one launch (start us, length us, event | category | flops | bytes accessed | tf_op | source)
XLA Modules:
  0.0 83.4 jit_solution(4318296195914266825)
XLA Ops:
  0.0 81.8 %whole.1 = bf16[64,2048]{1,0:T(8,128)(2,1)} custom-call(bf16[512,2048]{1,0:T(8,128)(2,1)} %refs_0_.1, bf16[8,128,2048]{2,1,0:T(8,128)(2,1)} %refs_1_.1, bf16[2048,256]{1,0:T(8,128)(2,1)} %refs_2_.1, bf16[2048,256]{1,0:T(8,128)(2,1)} %refs_3_.1, bf16[2048,256]{1,0:T(8,128)(2,1)} %refs_4_.1, bf16[2048,128]{1,0:T(8,128)(2,1)} %refs_5_.1, ...), custom_call_target="tpu_custom_call" | custom-call | tf_op jit(solution)/shard_map/whole/pallas_call | solution.py:647
  81.8 1.7 %copy.18 = bf16[64,2048]{1,0:T(8,128)(2,1)} copy(bf16[64,2048]{1,0:T(8,128)(2,1)} %whole.1) | data formatting | bytes 524288

commit v4 on v3

--- a/solution.py
+++ b/solution.py
@@ -14,7 +14,8 @@
 LANES = 128
 EPS = 1e-06
 EMPTY = -1e30
-BACKLOG = {6: 9.0, 7: 0.8, 8: 0.15, 9: 0.15}
+BACKLOG = {6: 1.5, 7: 1.5, 8: 0.8, 9: 0.3}
+GATE = {3: 3, 4: 3}
 MESH = pl.DeviceIdType.MESH
 F32 = jnp.float32
 BF16 = jnp.bfloat16
@@ -91,11 +92,11 @@
 def step_plan(k):
     plan = Plan()
     ring, half, groups, xhalf = k.ring, k.half, k.groups, k.xhalf
-    hop_late, far_late, q_wire, y_wire, x_wire = 2.4, 0.75, 1.4, 0.72, 1.4
+    hop_late, far_late, q_wire, y_wire, x_wire = 2.6, 0.75, 1.4, 0.72, 1.4
     for g in range(groups):
         plan.add(
             ("q", g), functools.partial(k.queries, g), 0.76, 1, [("q", g - 1)] if g else [],
-            sends=[(("q", side, 1, g), ("y", side), q_wire, hop_late) for side in range(2)],
+            sends=[(("q", side, 1, h), ("y", side), q_wire, hop_late) for side, h in k.first_sends(g)],
         )
     for hop in range(1, half + 1):
         for g in range(groups):
@@ -123,12 +124,13 @@
             hands = [("hand", 1 if rel < half else 0, hop, g) for g in range(groups)]
         else:
             hands = []
-        plan.add(("slots", rel), functools.partial(k.attend, rel), 0.6, 19 - hop, [("here",)] + hands)
+        plan.add(("slots", rel), functools.partial(k.attend, rel), 0.62, 19 - hop, [("here",)] + hands)
         plan.add(("attend", rel), functools.partial(k.join, rel), 0.3, 1, [("slots", rel)])
+    last_hands = [("hand", 0 if g < groups // 2 else 1, half - 1, g) for g in range(groups)]
     for rel in range(1, ring):
         hop = min(rel, ring - rel)
         plan.add(
-            ("direct", rel), functools.partial(k.direct, rel), 0.04, 2, [("attend", rel)],
+            ("direct", rel), functools.partial(k.direct, rel), 0.04, 2, [("attend", rel)] + last_hands,
             sends=[(("direct", ring - rel), ("y", 0 if rel <= half else 1), y_wire, hop_late + far_late * (hop - 1), hop)],
         )
     for c, chunk in enumerate(k.chunks[1:], 1):
@@ -141,6 +143,8 @@
                 )
             for side in range(2):
                 far = k.start_of(side, p)
+                gate = GATE.get(c, 0)
+                gated = [("y", side, q, gate) for q in k.chunks[c - 1]] if gate else []
                 for d in range(far, 0, -1):
                     rel = d if side == 0 else ring - d
                     gets = [] if d == far else [("y", side, p, d)]
@@ -149,7 +153,7 @@
                     plan.add(
                         ("y", side, p, d),
                         functools.partial(k.y_start if d == far else k.y_stage, side, p, d), 0.04 if d == far else 0.06,
-                        5 + c, [("attend", rel)], gets=gets,
+                        5 + c, [("attend", rel)] + (gated if d == far else []), gets=gets,
                         sends=[(("y", side, p, d - 1), ("y", side), y_wire, hop_late)],
                     )
     for g in range(groups):
@@ -198,6 +202,7 @@
         self.core, self.y_me = lax.rem(self.me, CORES), self.me // CORES
         self.partner = self.me + 1 - 2 * self.core
         self.right, self.left = self.chip(1), self.chip(self.ring - 1)
+        self.results = []
         self.waiting, self.unused, self.loads, self.clock = [], list(range(refs["send_sem"].shape[0])), [], 0.0
         self.early = 2
         self.places = order_of(n_tp)
@@ -318,8 +323,17 @@
         if g == 0:
             with jax.named_scope("entry"):
                 self.entered()
-        for side, rel, who in ((0, self.ring - 1, self.right), (1, 1, self.left)):
-            self.send(self.part(0, g), self.part(rel, g), self.q_recv.at[self.q_sem(side, 1, g)], st=who)
+        for side, h in self.first_sends(g):
+            rel, who = ((self.ring - 1, self.right), (1, self.left))[side]
+            self.send(self.part(0, h), self.part(rel, h), self.q_recv.at[self.q_sem(side, 1, h)], st=who)
+
+    def first_sends(self, g):
+        n = self.groups
+        if g == 0:
+            left = [0]
+        else:
+            left = [g] if g >= n // 2 else []
+        return [(0, g)] + [(1, h) for h in left] + ([(1, h) for h in range(1, n // 2)] if g == n - 1 else [])
 
     def hand_on(self, side, hop, g, on):
         rel = self.ring - hop if side == 0 else hop
@@ -540,7 +554,10 @@
             self.got(self.xdata.at[side, k, t], self.x_recv.at[self.x_sem(side, k, t)])
         if k == 0:
             y = y + self.xdata[0, k, t].astype(F32) + self.xdata[1, k, t].astype(F32)
-            self.out[:, at] = y.astype(BF16)
+            self.tile_out[t] = y.astype(BF16)
+            copy = pltpu.make_async_copy(self.tile_out.at[t], self.out.at[:, at], self.out_sem.at[t])
+            copy.start()
+            self.results.append(copy)
             return
         for side in outs:
             mine = y if len(chunk) == 1 else y[side * n : (side + 1) * n]
@@ -577,6 +594,8 @@
     with jax.named_scope(f"tail_{len(k.waiting)}"):
         while k.waiting:
             k.settle()
+        for copy in k.results:
+            copy.wait()
 
 
 def whole(ids, slots, blocks, per_block, big, small):
@@ -626,7 +645,9 @@
         "xdata": pltpu.VMEM((2, xhalf, tiles, mine, 512), BF16),
         "xfirst": pltpu.VMEM((tiles, mine, 512), BF16),
         "load_sem": dma((7 + groups + passages + len(small) + 1,)),
-        "send_sem": dma((48,)),
+        "tile_out": pltpu.VMEM((tiles, mine, 512), BF16),
+        "out_sem": dma((tiles,)),
+        "send_sem": dma((40,)),
         "q_recv": dma((2 * ((half - 1) * groups + groups // 2),)),
         "kv_recv": dma((2,)),
         "t_recv": dma((1,)),
@@ -643,12 +664,11 @@
     names = list(big) + list(small) + ["ids_hbm", "out"] + list(scratch)
     shapes = [s for n, s in scratch.items() if n != "qall"]
     shapes += [pltpu.VMEM((blocks, block_len, HD), BF16) for _ in range(ring)]
-    vmem = pl.BlockSpec(memory_space=pltpu.VMEM)
     return pl.pallas_call(
         functools.partial(whole_kernel, names, n_st, n_tp, slots, blocks, per_block),
         out_shape=jax.ShapeDtypeStruct((mine, width), BF16),
         in_specs=[pl.BlockSpec(memory_space=pltpu.HBM)] * (len(big) + len(small) + 1),
-        out_specs=vmem,
+        out_specs=pl.BlockSpec(memory_space=pltpu.HBM),
         scratch_shapes=shapes,
         compiler_params=pltpu.CompilerParams(
             collective_id=0, has_side_effects=True, vmem_limit_bytes=66_000_000

time: 83.6 us -> 84.1 us (level)
  no operation moved by 1% of the time
where the time goes in v4:
time: 84.1 us; the launch traced here: 83.5 us
  Pallas kernels  81.8 us (97%)
  local copies, waits for them, and re-layouts  1.67 us (2%)
    pallas_call x1, Pallas kernels, whole(): pl.pallas_call(functools.partial(whole_kernel, names, n_st, n_tp, slots,...  81.8 us

profile of v4, /device:TPU:528, one launch (start us, length us, event | category | flops | bytes accessed | tf_op | source)
XLA Modules:
  0.0 83.5 jit_solution(9691099661614239023)
XLA Ops:
  0.0 81.8 %whole.1 = bf16[64,2048]{1,0:T(8,128)(2,1)} custom-call(bf16[512,2048]{1,0:T(8,128)(2,1)} %refs_0_.1, bf16[8,128,2048]{2,1,0:T(8,128)(2,1)} %refs_1_.1, bf16[2048,256]{1,0:T(8,128)(2,1)} %refs_2_.1, bf16[2048,256]{1,0:T(8,128)(2,1)} %refs_3_.1, bf16[2048,256]{1,0:T(8,128)(2,1)} %refs_4_.1, bf16[2048,128]{1,0:T(8,128)(2,1)} %refs_5_.1, ...), custom_call_target="tpu_custom_call" | custom-call | tf_op jit(solution)/shard_map/whole/pallas_call | solution.py:667
  81.8 1.7 %copy.18 = bf16[64,2048]{1,0:T(8,128)(2,1)} copy(bf16[64,2048]{1,0:T(8,128)(2,1)} %whole.1) | data formatting | bytes 524288

commit v5 on v3

--- a/solution.py
+++ b/solution.py
@@ -246,6 +246,12 @@
         return self.start_cw[p] if side == 0 else 2 * self.half - 1 - self.start_cw[p]
 
     def enter(self):
+        barrier = pltpu.get_barrier_semaphore()
+        for d in range(1, self.ring):
+            pl.semaphore_signal(barrier, inc=1, device_id={"st": self.chip(d)}, device_id_type=MESH)
+        pl.semaphore_signal(barrier, inc=1, device_id={"st": self.partner}, device_id_type=MESH)
+        for d in range(1, self.n_tp):
+            pl.semaphore_signal(barrier, inc=1, device_id={"tp": self.column(d)}, device_id_type=MESH)
         small = lambda name: self.load(getattr(self, name + "_hbm"), getattr(self, name))
         self.first_loads = [small("qgain"), self.load(self.wq_hbm, self.wq)]
         rows = lambda g: pl.ds(g * 128, 128)
@@ -261,12 +267,6 @@
             self.load(self.gg_hbm, self.wglu.at[:, pl.ds(LANES, LANES)]),
         ]
         self.out_loads = [small("blend"), self.load(self.attn_hbm, self.attn), self.load(self.mix_hbm, self.mix)]
-        barrier = pltpu.get_barrier_semaphore()
-        for d in range(1, self.ring):
-            pl.semaphore_signal(barrier, inc=1, device_id={"st": self.chip(d)}, device_id_type=MESH)
-        pl.semaphore_signal(barrier, inc=1, device_id={"st": self.partner}, device_id_type=MESH)
-        for d in range(1, self.n_tp):
-            pl.semaphore_signal(barrier, inc=1, device_id={"tp": self.column(d)}, device_id_type=MESH)
         s = self.slots
         self.outs[s] = jnp.zeros(self.outs.shape[1:], BF16)
         self.ml[s, 0:1] = jnp.full((1, LANES), EMPTY, F32)
@@ -626,7 +626,7 @@
         "xdata": pltpu.VMEM((2, xhalf, tiles, mine, 512), BF16),
         "xfirst": pltpu.VMEM((tiles, mine, 512), BF16),
         "load_sem": dma((7 + groups + passages + len(small) + 1,)),
-        "send_sem": dma((48,)),
+        "send_sem": dma((32,)),
         "q_recv": dma((2 * ((half - 1) * groups + groups // 2),)),
         "kv_recv": dma((2,)),
         "t_recv": dma((1,)),

time: 83.6 us -> 83.5 us (level)
  no operation moved by 1% of the time
where the time goes in v5:
time: 83.5 us; the launch traced here: 83.4 us
  Pallas kernels  81.7 us (98%)
  local copies, waits for them, and re-layouts  1.67 us (2%)
    pallas_call x1, Pallas kernels, whole(): pl.pallas_call(functools.partial(whole_kernel, names, n_st, n_tp, slots,...  81.7 us
    unnamed x1, local copies, waits for them, and re-layouts  1.67 us

profile of v5, /device:TPU:528, one launch (start us, length us, event | category | flops | bytes accessed | tf_op | source)
XLA Modules:
  0.0 83.4 jit_solution(9710204615521606328)
XLA Ops:
  0.0 81.7 %whole.1 = bf16[64,2048]{1,0:T(8,128)(2,1)} custom-call(bf16[512,2048]{1,0:T(8,128)(2,1)} %refs_0_.1, bf16[8,128,2048]{2,1,0:T(8,128)(2,1)} %refs_1_.1, bf16[2048,256]{1,0:T(8,128)(2,1)} %refs_2_.1, bf16[2048,256]{1,0:T(8,128)(2,1)} %refs_3_.1, bf16[2048,256]{1,0:T(8,128)(2,1)} %refs_4_.1, bf16[2048,128]{1,0:T(8,128)(2,1)} %refs_5_.1, ...), custom_call_target="tpu_custom_call" | custom-call | tf_op jit(solution)/shard_map/whole/pallas_call | solution.py:647
  81.7 1.7 %copy.18 = bf16[64,2048]{1,0:T(8,128)(2,1)} copy(bf16[64,2048]{1,0:T(8,128)(2,1)} %whole.1) | data formatting | bytes 524288
